TPU v7x, 32 devices: a whole 2x2x4 slice. The times are simulated.
32 devices in a mesh: sp: 8 (over z, y), tp: 4 (over x, core).
Axes of the slice: x: 2, y: 2, z: 4, core: 2. Of those that a mesh axis runs over, the one named last changes fastest.
Arguments:
- resid: bfloat16 [6144, 2048], P(('sp', 'tp')), may hold values from -6 to 6
- query: bfloat16 [6144, 1024], P('sp', 'tp'), may hold values from -6 to 6
- keys: bfloat16 [6144, 1024], P('sp', 'tp'), may hold values from -6 to 6
- values: bfloat16 [6144, 1024], P('sp', 'tp'), may hold values from -6 to 6
- out_gate: bfloat16 [6144, 1024], P(('sp', 'tp')), may hold values from -6 to 6
- forget_pre: float32 [4, 6144], P('tp', 'sp'), may hold values from 0 to 16
- input_pre: float32 [4, 6144], P('tp', 'sp'), may hold values from -4 to 130
- head_gain: float32 [1024], replicated, may hold values from 0.1 to 1.9
- out_proj: bfloat16 [1024, 2048], replicated, may hold values from -0.1875 to 0.1875
- ffn_gain: float32 [2048], replicated, may hold values from 0.1 to 1.9
- routes: int32 [6144, 2], P(('sp', 'tp')), may hold values from 0 to 7, all different within a row; in each aligned block of 96 rows (0 to 95, 96 to 191, ...) at most 48 rows name the same one
- route_scores: float32 [6144, 2], P(('sp', 'tp')), may hold values from 0.1 to 1
- w_gate: bfloat16 [8, 2048, 512], P('sp'), may hold values from -0.125 to 0.125
- w_up: bfloat16 [8, 2048, 512], P('sp'), may hold values from -0.125 to 0.125
- w_down: bfloat16 [8, 512, 2048], P('sp'), may hold values from -0.25 to 0.25
Outputs:
- layer_out: bfloat16 [6144, 2048], P(('sp', 'tp'))
Inputs may be any that keep to these rules, and one draw needn't show every extreme that they name: `routes`: each row names 2 different experts; in each aligned block of 96 rows no expert is named by more than 48 rows, a bound that some block reaches.
All inputs are finite; a program needn't handle non-finite values.
Results may differ from a plain program's by a relative error of at most 0.0095.
Values may be sent and summed in bfloat16 or wider, within the bound.
A program may use at most 128 MiB of HBM per device.

v0:
```python
import functools

import jax
import jax.numpy as jnp
from jax import lax
from jax.experimental import pallas as pl
from jax.experimental.pallas import tpu as pltpu
from jax.sharding import PartitionSpec as P

BLOCK = 64


EPS = 1e-06
FLOOR_LOG = -1e30
HIGHEST = lax.Precision.HIGHEST


EXTRA = 8
VMEM_LIMIT = 56 * 1024 * 1024


def col_mask(first_row, rows, cols):
    row = lax.broadcasted_iota(jnp.int32, (rows, cols), 0) + first_row
    col = lax.broadcasted_iota(jnp.int32, (rows, cols), 1)
    return row, col


def split_two(a):
    high = a.astype(jnp.bfloat16)
    return high, (a - high.astype(jnp.float32)).astype(jnp.bfloat16)


def log_rows(forget_ref, input_ref):
    pre = forget_ref[...]
    log_forget = jnp.minimum(pre, 0.0) - jnp.log1p(jnp.exp(-jnp.abs(pre)))
    seq_len = pre.shape[1]
    row, col = col_mask(0, seq_len, seq_len)
    upper = jnp.where(row <= col, 1.0, 0.0).astype(jnp.bfloat16)
    one, rest = split_two(log_forget)
    two, three = split_two(log_forget - one.astype(jnp.float32))
    stacked = jnp.concatenate([one, two, three, jnp.zeros((13, seq_len), jnp.bfloat16)], axis=0)
    sums = jnp.dot(stacked, upper, preferred_element_type=jnp.float32)
    cum_row = sums[0:1] + sums[1:2] + sums[2:3]
    return log_forget, cum_row, input_ref[...] - cum_row


def cell_state_kernel(k_ref, v_ref, forget_ref, input_ref, state_ref):
    width = k_ref.shape[1]
    seq_len = k_ref.shape[0]
    log_forget, cum_row, gap_row = log_rows(forget_ref, input_ref)
    total = jnp.sum(log_forget, axis=1, keepdims=True)
    top = jnp.max(gap_row, axis=1, keepdims=True)
    keep_row = jnp.exp(gap_row - top) * width ** (-0.5)
    k_turned = k_ref[...].astype(jnp.float32).T
    weighted = k_turned * keep_row
    high, low = split_two(weighted)
    v = v_ref[...]
    state_ref[0:width, :] = jnp.dot(high, v, preferred_element_type=jnp.float32) + jnp.dot(
        low, v, preferred_element_type=jnp.float32
    )
    vector = jnp.dot(
        jnp.broadcast_to(keep_row, (8, seq_len)),
        k_ref[...].astype(jnp.float32),
        precision=HIGHEST,
        preferred_element_type=jnp.float32,
    )[0:1]
    lanes = jnp.zeros((1, width), jnp.float32)
    state_ref[width : width + EXTRA, :] = jnp.concatenate(
        [vector, lanes + total, lanes + total + top, jnp.zeros((EXTRA - 3, width), jnp.float32)],
        axis=0,
    )


def cell_local_kernel(q_ref, k_ref, v_ref, forget_ref, input_ref, num_ref, aux_ref, *, tile):
    seq_len, width = q_ref.shape
    log_forget, cum_row, gap_row = log_rows(forget_ref, input_ref)
    for first in range(0, seq_len, tile):
        span = first + tile
        row, col = col_mask(first, tile, span)
        causal = col <= row
        own = (col // BLOCK) == (row // BLOCK)
        gap = jnp.where(causal, gap_row[:, :span], -jnp.inf)
        top = jnp.max(gap, axis=1, keepdims=True)
        cum = jnp.sum(jnp.where(causal, log_forget[:, :span], 0.0), axis=1, keepdims=True)
        scores = lax.dot_general(
            q_ref[first:span, :],
            k_ref[0:span, :],
            (((1,), (1,)), ((), ())),
            preferred_element_type=jnp.float32,
        ) * width ** (-0.5)
        weights = scores * jnp.exp(gap - top)
        high = weights.astype(jnp.bfloat16)
        high_float = high.astype(jnp.float32)
        low_float = jnp.where(own, 0.0, weights - high_float)
        v = v_ref[0:span, :]
        num_ref[first:span, :] = jnp.dot(high, v, preferred_element_type=jnp.float32) + jnp.dot(
            low_float.astype(jnp.bfloat16), v, preferred_element_type=jnp.float32
        )
        den = jnp.sum(high_float + low_float, axis=1, keepdims=True)
        lane = lax.broadcasted_iota(jnp.int32, (tile, 128), 1)
        aux_ref[first:span, :] = jnp.where(lane == 0, den, jnp.where(lane == 1, top, cum))


def cell_join_kernel(q_ref, num_ref, aux_ref, states_ref, rows_ref, mat_ref, *, axis):
    width = q_ref.shape[1]
    place = lax.axis_index(axis)
    mat_ref[...] = jnp.zeros_like(mat_ref)

    def join(step, carry):
        vector, old_max = carry
        extra = states_ref[step, width : width + EXTRA, :]
        new_max, total = extra[2:3], extra[1:2]
        joined = jnp.maximum(total + old_max, new_max)
        keep_old = jnp.exp(total + old_max - joined)
        keep_new = jnp.exp(new_max - joined)
        mat_ref[...] = keep_old * mat_ref[...] + keep_new * states_ref[step, 0:width, :]
        return keep_old * vector + keep_new * extra[0:1], joined

    vector, far_max = lax.fori_loop(
        0,
        place,
        join,
        (jnp.zeros((1, width), jnp.float32), jnp.full((1, width), FLOOR_LOG, jnp.float32)),
    )
    aux = aux_ref[...]
    den, top, cum = aux[:, 0:1], aux[:, 1:2], aux[:, 2:3]
    far = far_max[:, 0:1]
    joined = jnp.maximum(top, far)
    keep_own = jnp.exp(top - joined)
    keep_far = jnp.exp(far - joined)
    q_float = q_ref[...].astype(jnp.float32)
    one, rest = split_two(mat_ref[...])
    two, three = split_two(mat_ref[...] - one.astype(jnp.float32))
    q = q_ref[...]
    far_num = (
        jnp.dot(q, one, preferred_element_type=jnp.float32)
        + jnp.dot(q, two, preferred_element_type=jnp.float32)
        + jnp.dot(q, three, preferred_element_type=jnp.float32)
    )
    far_den = jnp.sum(q_float * vector, axis=1, keepdims=True)
    numerator = keep_own * num_ref[...] + keep_far * far_num
    denominator = keep_own * den + keep_far * far_den
    divisor = jnp.maximum(jnp.abs(denominator), jnp.exp(-(cum + joined)))
    rows_ref[...] = (numerator / divisor).astype(rows_ref.dtype)


def run_cell(query, keys, values, forget_pre, input_pre):
    seq_len, width = query.shape
    params = pltpu.CompilerParams(vmem_limit_bytes=VMEM_LIMIT)
    state = pl.pallas_call(
        cell_state_kernel,
        out_shape=jax.ShapeDtypeStruct((width + EXTRA, width), jnp.float32),
        compiler_params=params,
        cost_estimate=pl.CostEstimate(flops=10**9, bytes_accessed=2**20, transcendentals=0),
        name="cell_state",
    )(keys, values, forget_pre, input_pre)
    cut = (width + EXTRA) // 3
    parts = [lax.all_gather(state[i * cut : (i + 1) * cut], "sp") for i in range(3)]
    gathered = jnp.concatenate(parts, axis=1)
    tile = 4 * BLOCK if seq_len % (4 * BLOCK) == 0 else BLOCK
    numerator, aux = pl.pallas_call(
        functools.partial(cell_local_kernel, tile=tile),
        out_shape=(
            jax.ShapeDtypeStruct((seq_len, width), jnp.float32),
            jax.ShapeDtypeStruct((seq_len, 128), jnp.float32),
        ),
        compiler_params=params,
        cost_estimate=pl.CostEstimate(flops=5 * 10**9, bytes_accessed=2**21, transcendentals=0),
        name="cell_local",
    )(query, keys, values, forget_pre, input_pre)
    rows = pl.pallas_call(
        functools.partial(cell_join_kernel, axis="sp"),
        out_shape=jax.ShapeDtypeStruct((seq_len, width), jnp.bfloat16),
        scratch_shapes=[pltpu.VMEM((width, width), jnp.float32)],
        compiler_params=params,
        name="cell_join",
    )(query, numerator, aux, gathered)
    return rows


def slot_select(expert_ids, expert_count, capacity):
    flat_ids = expert_ids.reshape(-1)
    one_hot = (flat_ids[:, None] == jnp.arange(expert_count, dtype=jnp.int32)[None, :]).astype(
        jnp.int32
    )
    slot_rank = jnp.sum((jnp.cumsum(one_hot, axis=0) - 1) * one_hot, axis=1)
    target = flat_ids * capacity + slot_rank
    return (
        jnp.arange(expert_count * capacity, dtype=jnp.int32)[:, None] == target[None, :]
    ).astype(jnp.bfloat16)


def exchange_kernel(send_ref, recv_ref, send_sems, recv_sems, own_sem, *, axis, count):
    place = lax.axis_index(axis)
    barrier = pltpu.get_barrier_semaphore()
    for step in range(1, count):
        peer = lax.rem(place + step, count)
        pl.semaphore_signal(
            barrier, inc=1, device_id={axis: peer}, device_id_type=pl.DeviceIdType.MESH
        )
    own = pltpu.make_async_copy(send_ref.at[place], recv_ref.at[place], own_sem)
    own.start()
    pl.semaphore_wait(barrier, count - 1)
    copies = []
    for step in range(1, count):
        peer = lax.rem(place + step, count)
        copy = pltpu.make_async_remote_copy(
            src_ref=send_ref.at[peer],
            dst_ref=recv_ref.at[place],
            send_sem=send_sems.at[step - 1],
            recv_sem=recv_sems.at[step - 1],
            device_id={axis: peer},
            device_id_type=pl.DeviceIdType.MESH,
        )
        copy.start()
        copies.append(copy)
    own.wait()
    for copy in copies:
        copy.wait()


def exchange(blocks, axis, collective_id):
    count = lax.axis_size(axis)
    grouped = blocks.reshape((count, -1) + blocks.shape[2:])
    out = pl.pallas_call(
        functools.partial(exchange_kernel, axis=axis, count=count),
        out_shape=jax.ShapeDtypeStruct(grouped.shape, grouped.dtype),
        in_specs=[pl.BlockSpec(memory_space=pl.ANY)],
        out_specs=pl.BlockSpec(memory_space=pl.ANY),
        scratch_shapes=[
            pltpu.SemaphoreType.DMA((count - 1,)),
            pltpu.SemaphoreType.DMA((count - 1,)),
            pltpu.SemaphoreType.DMA(()),
        ],
        compiler_params=pltpu.CompilerParams(collective_id=collective_id, has_side_effects=True),
        name="exchange",
    )(grouped)
    return out.reshape(blocks.shape)


def run_experts(arrived, w_gate, w_up, w_down, sources):
    local_count = w_gate.shape[0]
    grouped = arrived.reshape(sources, local_count, arrived.shape[1], arrived.shape[2])
    gate_pre = jnp.einsum("pesd,edf->pesf", grouped, w_gate, preferred_element_type=jnp.float32)
    up_pre = jnp.einsum("pesd,edf->pesf", grouped, w_up, preferred_element_type=jnp.float32)
    active = (jax.nn.silu(gate_pre) * up_pre).astype(jnp.bfloat16)
    result = jnp.einsum(
        "pesf,efd->pesd", active, w_down, preferred_element_type=jnp.float32
    ).astype(jnp.bfloat16)
    return result.reshape(arrived.shape)


def shards(
    resid,
    query,
    keys,
    values,
    out_gate,
    forget_pre,
    input_pre,
    head_gain,
    out_proj,
    ffn_gain,
    routes,
    route_scores,
    w_gate,
    w_up,
    w_down,
):
    head_width = query.shape[1]
    row_count, route_count = routes.shape
    sources = lax.axis_size("sp")
    local_experts = w_gate.shape[0]
    expert_count = local_experts * sources
    half_rows = row_count // 2
    capacity = max(2, 2 * half_rows * route_count // expert_count)
    route_weight = route_scores / jnp.sum(route_scores, axis=1, keepdims=True)
    cell_rows = run_cell(query, keys, values, forget_pre, input_pre)
    token_rows = lax.all_to_all(cell_rows, "tp", split_axis=0, concat_axis=1, tiled=True)
    cell_float = token_rows.astype(jnp.float32)
    headed = (
        cell_float
        * lax.rsqrt(jnp.mean(cell_float * cell_float, axis=1, keepdims=True) + EPS)
        * head_gain[None, :]
    )
    gated_out = (headed * jax.nn.sigmoid(out_gate.astype(jnp.float32))).astype(jnp.bfloat16)
    after_mix = resid.astype(jnp.float32) + jnp.dot(
        gated_out, out_proj, preferred_element_type=jnp.float32
    )
    normed_rows = (
        after_mix
        * lax.rsqrt(jnp.mean(after_mix * after_mix, axis=1, keepdims=True) + EPS)
        * ffn_gain[None, :]
    ).astype(jnp.bfloat16)
    selects = [
        slot_select(
            routes[half_idx * half_rows : (half_idx + 1) * half_rows], expert_count, capacity
        )
        for half_idx in range(2)
    ]

    def pack_rows(half_idx):
        selection = (
            selects[half_idx].reshape(expert_count * capacity, half_rows, route_count).sum(axis=2)
        )
        packed = jnp.dot(
            selection,
            normed_rows[half_idx * half_rows : (half_idx + 1) * half_rows],
            preferred_element_type=jnp.float32,
        )
        return packed.astype(jnp.bfloat16).reshape(expert_count, capacity, normed_rows.shape[1])

    send_rows = jnp.concatenate([pack_rows(0), pack_rows(1)], axis=1)
    finished = run_experts(
        exchange(send_rows, "sp", 1),
        w_gate,
        w_up,
        w_down,
        sources,
    )
    returned = exchange(finished, "sp", 2)
    answers = [returned[:, :capacity], returned[:, capacity:]]
    pieces = []
    for half_idx in range(2):
        gathered = lax.dot_general(
            selects[half_idx],
            answers[half_idx].reshape(expert_count * capacity, -1),
            (((0,), (0,)), ((), ())),
            preferred_element_type=jnp.float32,
        )
        weights_half = route_weight[half_idx * half_rows : (half_idx + 1) * half_rows]
        pieces.append(
            jnp.sum(gathered.reshape(half_rows, route_count, -1) * weights_half[:, :, None], axis=1)
        )
    return (after_mix + jnp.concatenate(pieces, axis=0)).astype(jnp.bfloat16)


def solution(mesh):
    placed = (
        P(("sp", "tp"), None),
        P("sp", "tp"),
        P("sp", "tp"),
        P("sp", "tp"),
        P(("sp", "tp"), None),
        P("tp", "sp"),
        P("tp", "sp"),
        P(),
        P(),
        P(),
        P(("sp", "tp"), None),
        P(("sp", "tp"), None),
        P("sp", None, None),
        P("sp", None, None),
        P("sp", None, None),
    )
    return jax.shard_map(
        shards, mesh=mesh, in_specs=placed, out_specs=P(("sp", "tp"), None), check_vma=False
    )
```

profile of v0, /device:TPU:12, one launch (start us, length us, event | category | flops | bytes accessed | tf_op | source)
XLA Modules:
  0.0 291.6 jit_solution(14992066985104962924)
XLA Ops:
  0.0 3.1 %cell_state.1 = f32[264,256]{1,0:T(8,128)} custom-call(bf16[768,256]{1,0:T(8,128)(2,1)} %k_ref.3, bf16[768,256]{1,0:T(8,128)(2,1)} %v_ref.3, f32[1,768]{1,0:T(1,128)} %forget_ref.3, f32[1,768]{1,0:T(1,128)} %input_ref.3), custom_call_target="tpu_custom_call" | custom-call | flops 1000000000 | bytes 1048576 | tf_op jit(solution)/shard_map/cell_state/pallas_call | solution.py:150
  3.1 1.0 fusion.38
  4.1 30.4 %all-gather = f32[704,256]{1,0:T(8,128)S(1)} all-gather(f32[88,256]{1,0:T(8,128)S(1)} %get-tuple-element.11), channel_id=2, replica_groups=mesh['sp'=8,'tp'=4] {'sp'}, dimensions={0}, use_global_device_ids=true | all-gather | bytes 811008 | tf_op jit(solution)/shard_map/all_gather | solution.py:158
  34.5 32.4 %all-gather.1 = f32[704,256]{1,0:T(8,128)S(1)} all-gather(f32[88,256]{1,0:T(8,128)S(1)} %get-tuple-element.13), channel_id=3, replica_groups=mesh['sp'=8,'tp'=4] {'sp'}, dimensions={0}, use_global_device_ids=true | all-gather | bytes 811008 | tf_op jit(solution)/shard_map/all_gather | solution.py:158
  66.8 31.0 %all-gather.2 = f32[704,256]{1,0:T(8,128)S(1)} all-gather(f32[88,256]{1,0:T(8,128)S(1)} %get-tuple-element.12), channel_id=4, replica_groups=mesh['sp'=8,'tp'=4] {'sp'}, dimensions={0}, use_global_device_ids=true | all-gather | bytes 811008 | tf_op jit(solution)/shard_map/all_gather | solution.py:158
  97.8 3.6 %cell_local.1 = (f32[768,256]{1,0:T(8,128)}, f32[768,128]{1,0:T(8,128)}) custom-call(bf16[768,256]{1,0:T(8,128)(2,1)} %q_ref.3, bf16[768,256]{1,0:T(8,128)(2,1)} %k_ref.3, bf16[768,256]{1,0:T(8,128)(2,1)} %v_ref.3, f32[1,768]{1,0:T(1,128)} %forget_ref.3, f32[1,768]{1,0:T(1,128)} %input_ref.3), custom_call_target="tpu_custom_call" | custom-call | flops 5000000000 | bytes 2097152 | tf_op jit(solution)/shard_map/cell_local/pallas_call | solution.py:161
  101.4 1.5 pad_maximum_fusion.1.states_ref
  102.9 4.2 %cell_join.1 = bf16[768,256]{1,0:T(8,128)(2,1)} custom-call(bf16[768,256]{1,0:T(8,128)(2,1)} %q_ref.3, f32[768,256]{1,0:T(8,128)} %get-tuple-element.7.num_ref, f32[768,128]{1,0:T(8,128)} %get-tuple-element.8.aux_ref, f32[8,264,256]{2,1,0:T(8,128)} %pad_maximum_fusion.1.states_ref), custom_call_target="tpu_custom_call" | custom-call | tf_op jit(solution)/shard_map/cell_join/pallas_call | solution.py:171
  107.2 3.8 %all-to-all-start = ((bf16[4,192,256]{2,1,0:T(8,128)(2,1)}), bf16[4,192,256]{2,1,0:T(8,128)(2,1)S(1)}, u32[]{:S(2)}, u32[]{:S(2)}) async-start(bf16[4,192,256]{2,1,0:T(8,128)(2,1)} %bitcast.97), calls=%async_computation | async-start | bytes 786432 | tf_op jit(solution)/shard_map/all_to_all | solution.py:279
  111.0 0.1 fusion.40
  111.0 0.1 copy.31
  111.1 0.1 reshape.176
  111.3 0.6 reduce-window.14
  111.9 0.2 slice_reduce_fusion.1
  112.1 0.1 add_bitcast_fusion.1
  112.3 0.1 reduce_sum.93
  112.4 0.1 copy.32
  112.5 0.1 eq.114
  112.7 0.6 reduce-window.16
  113.3 0.2 slice_reduce_fusion
  113.5 0.1 add_bitcast_fusion
  113.6 0.1 reduce_sum.97
  113.9 0.1 fusion.30
  114.1 0.1 iota_compare_fusion.3
  114.2 0.1 eq.109
  114.3 0.1 iota_compare_fusion
  114.4 0.1 eq.126
  114.5 0.1 fusion.29
  114.6 0.1 fusion.39
  114.7 3.4 %all-to-all-done = bf16[4,192,256]{2,1,0:T(8,128)(2,1)S(1)} async-done(((bf16[4,192,256]{2,1,0:T(8,128)(2,1)}), bf16[4,192,256]{2,1,0:T(8,128)(2,1)S(1)}, u32[]{:S(2)}, u32[]{:S(2)}) %all-to-all-start) | async-done | bytes 393248 | tf_op jit(solution)/shard_map/all_to_all | solution.py:279
  118.2 0.1 copy.33
  118.3 0.2 fusion.17
  118.5 0.8 copy-done.6
  119.3 3.5 %multiply_reduce_fusion = (f32[192]{0:T(256)S(1)}, f32[192,2048]{1,0:T(8,128)S(1)}) fusion(bf16[1024,2048]{1,0:T(8,128)(2,1)} %param.23, bf16[192,1024]{1,0:T(8,128)(2,1)S(1)} %copy-done.7, f32[192,1024]{1,0:T(8,128)S(1)} %bitcast.98, f32[1024]{0:T(1024)S(1)} %copy-done.8, f32[192]{0:T(256)S(1)} %add_rsqrt_fusion.1, bf16[192,2048]{1,0:T(8,128)(2,1)S(1)} %copy-done.6), kind=kOutput, calls=%fused_computation.23 | convolution fusion | flops 808451904 | bytes 7738880 | tf_op jit(solution)/shard_map/dot_general | solution.py:287
  122.8 0.2 multiply_convert_fusion
  123.0 0.6 convolution_convert_fusion.2
  123.6 0.3 copy-done.1
  123.9 0.6 convolution_convert_fusion.1
  124.5 2.1 pad_maximum_fusion.send_ref
  126.6 74.4 %exchange.2 = bf16[8,96,2048]{2,1,0:T(8,128)(2,1)} custom-call(bf16[8,96,2048]{2,1,0:T(8,128)(2,1)} %pad_maximum_fusion.send_ref), custom_call_target="tpu_custom_call" | custom-call | tf_op jit(solution)/shard_map/exchange/pallas_call | solution.py:225
  201.0 5.6 %fusion.3 = f32[8,96,512]{2,1,0:T(8,128)} fusion(bf16[8,96,2048]{2,1,0:T(8,128)(2,1)} %exchange.2, bf16[1,2048,512]{2,1,0:T(8,128)(2,1)} %param.27), kind=kOutput, calls=%fused_computation.11 | convolution fusion | flops 1610612736 | bytes 6815744 | tf_op jit(solution)/shard_map/pesd,edf->pesf/dot_general | solution.py:244
  206.6 8.2 %convolution_convert_fusion.send_ref = bf16[8,96,2048]{2,1,0:T(8,128)(2,1)} fusion(bf16[1,512,2048]{2,1,0:T(8,128)(2,1)S(1)} %copy-done, bf16[8,96,2048]{2,1,0:T(8,128)(2,1)} %exchange.2, bf16[1,2048,512]{2,1,0:T(8,128)(2,1)} %param.28, f32[8,96,512]{2,1,0:T(8,128)} %fusion.3), kind=kOutput, calls=%fused_computation | convolution fusion | flops 3225157632 | bytes 12058624 | tf_op jit(solution)/shard_map/pesf,efd->pesd/dot_general | solution.py:247
  214.8 71.4 %exchange.3 = bf16[8,96,2048]{2,1,0:T(8,128)(2,1)} custom-call(bf16[8,96,2048]{2,1,0:T(8,128)(2,1)} %convolution_convert_fusion.send_ref), custom_call_target="tpu_custom_call" | custom-call | tf_op jit(solution)/shard_map/exchange/pallas_call | solution.py:225
  286.2 2.3 fusion.37
  288.5 0.6 fusion.12
  289.1 0.6 fusion.13
  289.7 0.8 copy-done.2
  290.5 1.1 fusion.5
  (36 shorter events, 0.5 us)
Async XLA Ops:
  0.0 206.6 %copy-start = (bf16[1,512,2048]{2,1,0:T(8,128)(2,1)S(1)}, bf16[1,512,2048]{2,1,0:T(8,128)(2,1)}, u32[]{:S(2)}) copy-start(bf16[1,512,2048]{2,1,0:T(8,128)(2,1)} %param.29) | copy-start | bytes 6291460
  102.9 8.0 %copy-start.5 = (s32[192,2]{0,1:T(2,128)S(1)}, s32[192,2]{0,1:T(2,128)}, u32[]{:S(2)}) copy-start(s32[192,2]{0,1:T(2,128)} %param.25) | copy-start | bytes 4612
  107.2 7.1 %copy-start.4 = (f32[192,2]{0,1:T(2,128)S(1)}, f32[192,2]{0,1:T(2,128)}, u32[]{:S(2)}) copy-start(f32[192,2]{0,1:T(2,128)} %param.26) | copy-start | bytes 4612
  107.2 11.0 %all-to-all-start = ((bf16[4,192,256]{2,1,0:T(8,128)(2,1)}), bf16[4,192,256]{2,1,0:T(8,128)(2,1)S(1)}, u32[]{:S(2)}, u32[]{:S(2)}) async-start(bf16[4,192,256]{2,1,0:T(8,128)(2,1)} %bitcast.97), calls=%async_computation | async-start | bytes 786432 | tf_op jit(solution)/shard_map/all_to_all | solution.py:279
  114.7 3.8 %copy-start.7 = (bf16[192,1024]{1,0:T(8,128)(2,1)S(1)}, bf16[192,1024]{1,0:T(8,128)(2,1)}, u32[]{:S(2)}) copy-start(bf16[192,1024]{1,0:T(8,128)(2,1)} %param.19) | copy-start | bytes 1179652
  114.7 3.8 %copy-start.8 = (f32[1024]{0:T(1024)S(1)}, f32[1024]{0:T(1024)}, u32[]{:S(2)}) copy-start(f32[1024]{0:T(1024)} %param.22) | copy-start | bytes 12292
  118.2 1.1 copy-start.6
  119.3 3.5 %copy-start.3 = (f32[2048]{0:T(1024)S(1)}, f32[2048]{0:T(1024)}, u32[]{:S(2)}) copy-start(f32[2048]{0:T(1024)} %param.24) | copy-start | bytes 24580
  122.8 1.2 copy-start.1
  289.1 1.4 copy-start.2
where the time goes:
time: 292 us
  Pallas kernels  157 us (54%)
  blocking collectives  93.7 us (32%)
  matrix products  19.6 us (7%)
  other arithmetic  7.08 us (2%)
  local copies, waits for them, and re-layouts  6.91 us (2%)
  starting transfers between devices  3.77 us (1%)
  waiting for transfers between devices  3.43 us (1%)
    pallas_call x2, Pallas kernels, exchange(): pl.pallas_call(functools.partial(exchange_kernel, axis=axis, count=count)...  146 us
    all_gather x3, blocking collectives, run_cell(): lax.all_gather(state[i * cut:(i + 1) * cut], 'sp')  93.7 us
    dot_general x1, matrix products, run_experts(): jnp.einsum('pesf,efd->pesd', active, w_down, preferred_element_type=jnp.f...  8.17 us
  transfers between devices with their start and end apart: 1, of which 1 were waited for; matrix products, arithmetic and copies ran while one was open for 1% of the time, Pallas kernels for 0%

commit v1 on v0

--- a/solution.py
+++ b/solution.py
@@ -178,6 +178,259 @@
     return rows
 
 
+def sp_tp_barrier(barrier, counts):
+    total = 0
+    for axis, count in counts.items():
+        place = lax.axis_index(axis)
+        for step in range(1, count):
+            pl.semaphore_signal(
+                barrier,
+                inc=1,
+                device_id={axis: lax.rem(place + step, count)},
+                device_id_type=pl.DeviceIdType.MESH,
+            )
+        total += count - 1
+    return total
+
+
+def cell_kernel(
+    q_ref,
+    k_ref,
+    v_ref,
+    forget_ref,
+    input_ref,
+    out_ref,
+    state_ref,
+    piece_ref,
+    extra_ref,
+    prefix_ref,
+    mat_ref,
+    num_ref,
+    aux_ref,
+    rows_ref,
+    send_sems,
+    recv_sems,
+    extra_send_sems,
+    extra_recv_sems,
+    back_send_sems,
+    back_recv_sems,
+    turn_send_sems,
+    turn_recv_sems,
+    own_sem,
+    *,
+    count,
+    heads,
+    tile,
+):
+    seq_len, width = q_ref.shape
+    cut = width // count
+    place = lax.axis_index("sp")
+    head = lax.axis_index("tp")
+    barrier = pltpu.get_barrier_semaphore()
+    greeted = sp_tp_barrier(barrier, {"sp": count, "tp": heads})
+    log_forget, cum_row, gap_row = log_rows(forget_ref, input_ref)
+    total = jnp.sum(log_forget, axis=1, keepdims=True)
+    best = jnp.max(gap_row, axis=1, keepdims=True)
+    keep_row = jnp.exp(gap_row - best) * width ** (-0.5)
+    weighted = k_ref[...].astype(jnp.float32).T * keep_row
+    high, low = split_two(weighted)
+    v_all = v_ref[...]
+    state_ref[0:width, :] = jnp.dot(high, v_all, preferred_element_type=jnp.float32) + jnp.dot(
+        low, v_all, preferred_element_type=jnp.float32
+    )
+    vector = jnp.dot(
+        jnp.broadcast_to(keep_row, (8, seq_len)),
+        k_ref[...].astype(jnp.float32),
+        precision=HIGHEST,
+        preferred_element_type=jnp.float32,
+    )[0:1]
+    lanes = jnp.zeros((1, width), jnp.float32)
+    state_ref[width : width + EXTRA, :] = jnp.concatenate(
+        [vector, lanes + total, lanes + total + best, jnp.zeros((EXTRA - 3, width), jnp.float32)],
+        axis=0,
+    )
+    pl.semaphore_wait(barrier, greeted)
+    sends = []
+    for step in range(1, count):
+        peer = lax.rem(place + step, count)
+        extra_copy = pltpu.make_async_remote_copy(
+            src_ref=state_ref.at[pl.ds(width, EXTRA)],
+            dst_ref=extra_ref.at[place],
+            send_sem=extra_send_sems.at[step - 1],
+            recv_sem=extra_recv_sems.at[step - 1],
+            device_id={"sp": peer},
+            device_id_type=pl.DeviceIdType.MESH,
+        )
+        piece_copy = pltpu.make_async_remote_copy(
+            src_ref=state_ref.at[pl.ds(pl.multiple_of(peer * cut, cut), cut)],
+            dst_ref=piece_ref.at[place],
+            send_sem=send_sems.at[step - 1],
+            recv_sem=recv_sems.at[step - 1],
+            device_id={"sp": peer},
+            device_id_type=pl.DeviceIdType.MESH,
+        )
+        extra_copy.start()
+        piece_copy.start()
+        sends += [extra_copy, piece_copy]
+    extra_ref[place] = state_ref[width : width + EXTRA, :]
+    piece_ref[place] = state_ref[pl.ds(pl.multiple_of(place * cut, cut), cut), :]
+
+    for first in range(0, seq_len, tile):
+        span = first + tile
+        row, col = col_mask(first, tile, span)
+        causal = col <= row
+        own = (col // BLOCK) == (row // BLOCK)
+        gap = jnp.where(causal, gap_row[:, :span], -jnp.inf)
+        top = jnp.max(gap, axis=1, keepdims=True)
+        cum = jnp.sum(jnp.where(causal, log_forget[:, :span], 0.0), axis=1, keepdims=True)
+        scores = lax.dot_general(
+            q_ref[first:span, :],
+            k_ref[0:span, :],
+            (((1,), (1,)), ((), ())),
+            preferred_element_type=jnp.float32,
+        ) * width ** (-0.5)
+        weights = scores * jnp.exp(gap - top)
+        high = weights.astype(jnp.bfloat16)
+        high_float = high.astype(jnp.float32)
+        low_float = jnp.where(own, 0.0, weights - high_float)
+        v = v_ref[0:span, :]
+        num_ref[first:span, :] = jnp.dot(high, v, preferred_element_type=jnp.float32) + jnp.dot(
+            low_float.astype(jnp.bfloat16), v, preferred_element_type=jnp.float32
+        )
+        den = jnp.sum(high_float + low_float, axis=1, keepdims=True)
+        lane = lax.broadcasted_iota(jnp.int32, (tile, 128), 1)
+        aux_ref[first:span, :] = jnp.where(lane == 0, den, jnp.where(lane == 1, top, cum))
+
+    for copy in sends:
+        copy.wait()
+
+    running = jnp.zeros((cut, width), jnp.float32)
+    vector = jnp.zeros((1, width), jnp.float32)
+    far_max = jnp.full((1, width), FLOOR_LOG, jnp.float32)
+    own_vector, own_max = vector, far_max
+    for step in range(count):
+        prefix_ref[step] = running
+        own_vector = jnp.where(place == step, vector, own_vector)
+        own_max = jnp.where(place == step, far_max, own_max)
+        if step < count - 1:
+            extra = extra_ref[step]
+            new_max, step_total = extra[2:3], extra[1:2]
+            joined = jnp.maximum(step_total + far_max, new_max)
+            keep_old = jnp.exp(step_total + far_max - joined)
+            keep_new = jnp.exp(new_max - joined)
+            running = keep_old * running + keep_new * piece_ref[step]
+            vector = keep_old * vector + keep_new * extra[0:1]
+            far_max = joined
+    backs = []
+    for step in range(1, count):
+        peer = lax.rem(place + step, count)
+        back = pltpu.make_async_remote_copy(
+            src_ref=prefix_ref.at[peer],
+            dst_ref=mat_ref.at[pl.ds(pl.multiple_of(place * cut, cut), cut)],
+            send_sem=back_send_sems.at[step - 1],
+            recv_sem=back_recv_sems.at[step - 1],
+            device_id={"sp": peer},
+            device_id_type=pl.DeviceIdType.MESH,
+        )
+        back.start()
+        backs.append(back)
+    mat_ref[pl.ds(pl.multiple_of(place * cut, cut), cut), :] = prefix_ref[place]
+
+    aux = aux_ref[...]
+    den, top, cum = aux[:, 0:1], aux[:, 1:2], aux[:, 2:3]
+    far = own_max[:, 0:1]
+    joined = jnp.maximum(top, far)
+    keep_own = jnp.exp(top - joined)
+    keep_far = jnp.exp(far - joined)
+    q_float = q_ref[...].astype(jnp.float32)
+    far_den = jnp.sum(q_float * own_vector, axis=1, keepdims=True)
+    denominator = keep_own * den + keep_far * far_den
+    divisor = jnp.maximum(jnp.abs(denominator), jnp.exp(-(cum + joined)))
+    for copy in backs:
+        copy.wait()
+    one, rest = split_two(mat_ref[...])
+    two, three = split_two(mat_ref[...] - one.astype(jnp.float32))
+    q = q_ref[...]
+    far_num = (
+        jnp.dot(q, one, preferred_element_type=jnp.float32)
+        + jnp.dot(q, two, preferred_element_type=jnp.float32)
+        + jnp.dot(q, three, preferred_element_type=jnp.float32)
+    )
+    numerator = keep_own * num_ref[...] + keep_far * far_num
+    rows_ref[...] = (numerator / divisor).astype(rows_ref.dtype)
+
+    share = seq_len // heads
+    columns = pl.ds(pl.multiple_of(head * width, width), width)
+    turns = []
+    for step in range(1, heads):
+        peer = lax.rem(head + step, heads)
+        turn = pltpu.make_async_remote_copy(
+            src_ref=rows_ref.at[pl.ds(pl.multiple_of(peer * share, share), share)],
+            dst_ref=out_ref.at[:, columns],
+            send_sem=turn_send_sems.at[step - 1],
+            recv_sem=turn_recv_sems.at[step - 1],
+            device_id={"tp": peer},
+            device_id_type=pl.DeviceIdType.MESH,
+        )
+        turn.start()
+        turns.append(turn)
+    own_copy = pltpu.make_async_copy(
+        rows_ref.at[pl.ds(pl.multiple_of(head * share, share), share)],
+        out_ref.at[:, columns],
+        own_sem,
+    )
+    own_copy.start()
+    own_copy.wait()
+    for turn in turns:
+        turn.wait()
+
+
+def run_cell_scan(query, keys, values, forget_pre, input_pre):
+    seq_len, width = query.shape
+    count, heads = lax.axis_size("sp"), lax.axis_size("tp")
+    tile = 4 * BLOCK if seq_len % (4 * BLOCK) == 0 else BLOCK
+    cut = width // count
+    vmem = pl.BlockSpec(memory_space=pltpu.VMEM)
+    dma = pltpu.SemaphoreType.DMA
+    return pl.pallas_call(
+        functools.partial(cell_kernel, count=count, heads=heads, tile=tile),
+        out_shape=jax.ShapeDtypeStruct((seq_len // heads, heads * width), jnp.bfloat16),
+        in_specs=[vmem] * 5,
+        out_specs=vmem,
+        scratch_shapes=[
+            pltpu.VMEM((width + EXTRA, width), jnp.float32),
+            pltpu.VMEM((count, cut, width), jnp.float32),
+            pltpu.VMEM((count, EXTRA, width), jnp.float32),
+            pltpu.VMEM((count, cut, width), jnp.float32),
+            pltpu.VMEM((width, width), jnp.float32),
+            pltpu.VMEM((seq_len, width), jnp.float32),
+            pltpu.VMEM((seq_len, 128), jnp.float32),
+            pltpu.VMEM((seq_len, width), jnp.bfloat16),
+            dma((count - 1,)),
+            dma((count - 1,)),
+            dma((count - 1,)),
+            dma((count - 1,)),
+            dma((count - 1,)),
+            dma((count - 1,)),
+            dma((heads - 1,)),
+            dma((heads - 1,)),
+            dma(()),
+        ],
+        compiler_params=pltpu.CompilerParams(
+            vmem_limit_bytes=VMEM_LIMIT, collective_id=3, has_side_effects=True
+        ),
+        cost_estimate=pl.CostEstimate(flops=10**10, bytes_accessed=2**21, transcendentals=0),
+        name="cell",
+    )(query, keys, values, forget_pre, input_pre)
+
+
+def token_cell(query, keys, values, forget_pre, input_pre):
+    if query.shape[1] % (8 * lax.axis_size("sp")) == 0:
+        return run_cell_scan(query, keys, values, forget_pre, input_pre)
+    rows = run_cell(query, keys, values, forget_pre, input_pre)
+    return lax.all_to_all(rows, "tp", split_axis=0, concat_axis=1, tiled=True)
+
+
 def slot_select(expert_ids, expert_count, capacity):
     flat_ids = expert_ids.reshape(-1)
     one_hot = (flat_ids[:, None] == jnp.arange(expert_count, dtype=jnp.int32)[None, :]).astype(
@@ -275,8 +528,7 @@
     half_rows = row_count // 2
     capacity = max(2, 2 * half_rows * route_count // expert_count)
     route_weight = route_scores / jnp.sum(route_scores, axis=1, keepdims=True)
-    cell_rows = run_cell(query, keys, values, forget_pre, input_pre)
-    token_rows = lax.all_to_all(cell_rows, "tp", split_axis=0, concat_axis=1, tiled=True)
+    token_rows = token_cell(query, keys, values, forget_pre, input_pre)
     cell_float = token_rows.astype(jnp.float32)
     headed = (
         cell_float

time: 292 us -> 209 us (0.72)
  the two profiles are of different devices: /device:TPU:12 before, /device:TPU:13 now
where the time goes in v1:
time: 209 us
  Pallas kernels  172 us (82%)
  matrix products  22.7 us (11%)
  local copies, waits for them, and re-layouts  7.25 us (3%)
  other arithmetic  6.67 us (3%)
    pallas_call x2, Pallas kernels, exchange(): pl.pallas_call(functools.partial(exchange_kernel, axis=axis, count=count)...  145 us
    pallas_call x1, Pallas kernels, run_cell_scan(): pl.pallas_call(functools.partial(cell_kernel, count=count, heads=heads, t...  27.5 us
    dot_general x1, matrix products, run_experts(): jnp.einsum('pesf,efd->pesd', active, w_down, preferred_element_type=jnp.f...  8.18 us
    dot_general x1, matrix products, run_experts(): jnp.einsum('pesd,edf->pesf', grouped, w_gate, preferred_element_type=jnp....  5.56 us
    dot_general x2, matrix products, shards(): lax.dot_general(selects[half_idx], answers[half_idx].reshape(expert_count...  4.23 us

profile of v1, /device:TPU:13, one launch (start us, length us, event | category | flops | bytes accessed | tf_op | source)
XLA Modules:
  0.0 209.1 jit_solution(3073954204255885935)
XLA Ops:
  0.0 0.0 copy-start
  0.0 0.9 fusion.43
  0.9 0.1 copy.28
  1.0 0.1 reshape.171
  1.2 0.6 reduce-window.14
  1.8 0.2 slice_reduce_fusion.1
  2.0 0.1 add_bitcast_fusion.1
  2.1 0.1 reduce_sum.93
  2.3 0.1 copy.23
  2.4 0.1 fusion.34
  2.5 0.0 copy-start.6
  2.5 0.0 copy-start.7
  2.5 0.0 copy-start.8
  2.5 0.0 copy-start.9
  2.5 27.5 %cell.1 = bf16[192,1024]{1,0:T(8,128)(2,1)} custom-call(bf16[768,256]{1,0:T(8,128)(2,1)} %q_ref.1, bf16[768,256]{1,0:T(8,128)(2,1)} %k_ref.1, bf16[768,256]{1,0:T(8,128)(2,1)} %v_ref.1, f32[1,768]{1,0:T(1,128)} %forget_ref.1, f32[1,768]{1,0:T(1,128)} %input_ref.1), custom_call_target="tpu_custom_call" | custom-call | flops 10000000000 | bytes 2097152 | tf_op jit(solution)/shard_map/cell/pallas_call | solution.py:395
  30.0 1.2 fusion.17
  31.2 0.0 copy-done.6
  31.2 0.0 copy-done.7
  31.2 0.0 copy-start.4
  31.2 2.4 %multiply_reduce_fusion = (f32[192]{0:T(256)S(1)}, f32[192,2048]{1,0:T(8,128)S(1)}) fusion(bf16[1024,2048]{1,0:T(8,128)(2,1)S(1)} %copy-done.6, bf16[192,1024]{1,0:T(8,128)(2,1)} %cell.1, bf16[192,1024]{1,0:T(8,128)(2,1)S(1)} %copy-done.8, f32[1024]{0:T(1024)S(1)} %copy-done.9, f32[192]{0:T(256)S(1)} %add_rsqrt_fusion.1, bf16[192,2048]{1,0:T(8,128)(2,1)S(1)} %copy-done.7), kind=kOutput, calls=%fused_computation.22 | convolution fusion | flops 808648512 | bytes 7345664 | tf_op jit(solution)/shard_map/dot_general | solution.py:539
  33.6 0.2 multiply_convert_fusion
  33.8 1.7 convolution_convert_fusion.2
  35.6 0.1 copy.29
  35.7 0.1 eq.114
  35.9 0.7 reduce-window.16
  36.6 0.2 slice_reduce_fusion
  36.9 0.1 add_bitcast_fusion
  37.0 0.1 reduce_sum.97
  37.1 0.1 copy.25
  37.2 0.1 fusion.33
  37.3 0.6 convolution_convert_fusion.1
  37.9 0.7 copy-done.3
  38.6 2.1 pad_maximum_fusion.send_ref
  40.7 72.7 %exchange.2 = bf16[8,96,2048]{2,1,0:T(8,128)(2,1)} custom-call(bf16[8,96,2048]{2,1,0:T(8,128)(2,1)} %pad_maximum_fusion.send_ref), custom_call_target="tpu_custom_call" | custom-call | tf_op jit(solution)/shard_map/exchange/pallas_call | solution.py:478
  113.4 5.6 %fusion.3 = f32[8,96,512]{2,1,0:T(8,128)} fusion(bf16[8,96,2048]{2,1,0:T(8,128)(2,1)} %exchange.2, bf16[1,2048,512]{2,1,0:T(8,128)(2,1)} %param.27), kind=kOutput, calls=%fused_computation.10 | convolution fusion | flops 1610612736 | bytes 6815744 | tf_op jit(solution)/shard_map/pesd,edf->pesf/dot_general | solution.py:497
  119.0 8.2 %convolution_convert_fusion.send_ref = bf16[8,96,2048]{2,1,0:T(8,128)(2,1)} fusion(bf16[1,512,2048]{2,1,0:T(8,128)(2,1)S(1)} %copy-done, bf16[8,96,2048]{2,1,0:T(8,128)(2,1)} %exchange.2, bf16[1,2048,512]{2,1,0:T(8,128)(2,1)} %param.28, f32[8,96,512]{2,1,0:T(8,128)} %fusion.3), kind=kOutput, calls=%fused_computation | convolution fusion | flops 3225157632 | bytes 12058624 | tf_op jit(solution)/shard_map/pesf,efd->pesd/dot_general | solution.py:500
  127.1 72.1 %exchange.3 = bf16[8,96,2048]{2,1,0:T(8,128)(2,1)} custom-call(bf16[8,96,2048]{2,1,0:T(8,128)(2,1)} %convolution_convert_fusion.send_ref), custom_call_target="tpu_custom_call" | custom-call | tf_op jit(solution)/shard_map/exchange/pallas_call | solution.py:478
  199.2 0.0 copy-start.5
  199.2 4.0 %fusion.41 = (bf16[8,48,2048]{2,1,0:T(8,128)(2,1)}, bf16[8,48,2048]{2,1,0:T(8,128)(2,1)}) fusion(bf16[8,96,2048]{2,1,0:T(8,128)(2,1)} %exchange.3), kind=kLoop, calls=%fused_computation.72 | loop fusion | bytes 6291456 | tf_op jit(solution)/shard_map/slice | solution.py:574
  203.2 0.1 iota_compare_fusion.3
  203.3 0.1 eq.109
  203.4 0.0 copy-done.5
  203.5 0.1 fusion.42
  203.5 2.1 fusion.12
  205.6 0.1 iota_compare_fusion
  205.7 0.1 eq.126
  205.8 2.2 %fusion.13 = f32[96,2048]{1,0:T(8,128)S(1)} fusion(bf16[384,2048,1]{1,0,2:T(8,128)(2,1)} %bitcast.84, f32[96,2]{0,1:T(2,128)S(1)} %get-tuple-element.8, pred[96,2,384]{2,1,0:T(4,128)(4,1)S(1)} %eq.126), kind=kOutput, calls=%fused_computation.24 | convolution fusion | flops 302579712 | bytes 2433792 | tf_op jit(solution)/shard_map/dot_general | solution.py:577
  208.0 1.1 fusion.5
  (27 shorter events, 0.3 us)
Async XLA Ops:
  0.0 118.9 %copy-start = (bf16[1,512,2048]{2,1,0:T(8,128)(2,1)S(1)}, bf16[1,512,2048]{2,1,0:T(8,128)(2,1)}, u32[]{:S(2)}) copy-start(bf16[1,512,2048]{2,1,0:T(8,128)(2,1)} %param.29) | copy-start | bytes 6291460
  2.5 28.7 %copy-start.6 = (bf16[1024,2048]{1,0:T(8,128)(2,1)S(1)}, bf16[1024,2048]{1,0:T(8,128)(2,1)}, u32[]{:S(2)}) copy-start(bf16[1024,2048]{1,0:T(8,128)(2,1)} %param.23) | copy-start | bytes 12582916
  2.5 28.7 %copy-start.7 = (bf16[192,2048]{1,0:T(8,128)(2,1)S(1)}, bf16[192,2048]{1,0:T(8,128)(2,1)}, u32[]{:S(2)}) copy-start(bf16[192,2048]{1,0:T(8,128)(2,1)} %param.15) | copy-start | bytes 2359300
  2.5 28.7 %copy-start.8 = (bf16[192,1024]{1,0:T(8,128)(2,1)S(1)}, bf16[192,1024]{1,0:T(8,128)(2,1)}, u32[]{:S(2)}) copy-start(bf16[192,1024]{1,0:T(8,128)(2,1)} %param.19) | copy-start | bytes 1179652
  2.5 28.7 %copy-start.9 = (f32[1024]{0:T(1024)S(1)}, f32[1024]{0:T(1024)}, u32[]{:S(2)}) copy-start(f32[1024]{0:T(1024)} %param.22) | copy-start | bytes 12292
  31.2 2.4 %copy-start.4 = (f32[2048]{0:T(1024)S(1)}, f32[2048]{0:T(1024)}, u32[]{:S(2)}) copy-start(f32[2048]{0:T(1024)} %param.24) | copy-start | bytes 24580
  33.6 2.0 copy-start.1
  37.2 1.4 copy-start.3
  199.2 4.2 %copy-start.5 = (f32[192,2]{0,1:T(2,128)S(1)}, f32[192,2]{0,1:T(2,128)}, u32[]{:S(2)}) copy-start(f32[192,2]{0,1:T(2,128)} %param.26) | copy-start | bytes 4612
  205.8 2.2 %copy-start.2 = (f32[192,2048]{1,0:T(8,128)S(1)}, f32[192,2048]{1,0:T(8,128)}, u32[]{:S(2)}) copy-start(f32[192,2048]{1,0:T(8,128)} %copy-done.1) | copy-start | bytes 4718596

commit v2 on v1

--- a/solution.py
+++ b/solution.py
@@ -503,6 +503,401 @@
     return result.reshape(arrived.shape)
 
 
+def line_kernel(
+    rows_ref,
+    mix_ref,
+    info_ref,
+    gate_hbm,
+    up_hbm,
+    down_hbm,
+    out_ref,
+    gate_ref,
+    up_ref,
+    down_ref,
+    infos_ref,
+    held_ref,
+    cross_ref,
+    crossed_ref,
+    answer_ref,
+    done_ref,
+    batch_ref,
+    part_ref,
+    own_ref,
+    sum_ref,
+    load_sems,
+    info_send,
+    info_recv,
+    row_send,
+    row_recv,
+    cross_send,
+    cross_recv,
+    answer_send,
+    answer_recv,
+    sum_send,
+    sum_recv,
+    *,
+    line,
+    halves,
+    slots,
+):
+    place = lax.axis_index("sp")
+    here = place // 2
+    side = lax.rem(place, 2)
+    twin = place + 1 - 2 * side
+    units = line * halves
+    tokens = rows_ref.shape[1]
+    last = line - 1
+
+    def remote(src, dst, send, recv, peer):
+        return pltpu.make_async_remote_copy(
+            src_ref=src,
+            dst_ref=dst,
+            send_sem=send,
+            recv_sem=recv,
+            device_id={"sp": peer},
+            device_id_type=pl.DeviceIdType.MESH,
+        )
+
+    loads = [
+        pltpu.make_async_copy(src, dst, load_sems.at[i])
+        for i, (src, dst) in enumerate(
+            [(gate_hbm, gate_ref), (up_hbm, up_ref), (down_hbm, down_ref)]
+        )
+    ]
+    for load in loads:
+        load.start()
+
+    barrier = pltpu.get_barrier_semaphore()
+    for step in range(1, line):
+        pl.semaphore_signal(
+            barrier,
+            inc=1,
+            device_id={"sp": lax.rem(here + step, line) * 2 + side},
+            device_id_type=pl.DeviceIdType.MESH,
+        )
+    pl.semaphore_signal(
+        barrier, inc=1, device_id={"sp": twin}, device_id_type=pl.DeviceIdType.MESH
+    )
+    pl.semaphore_wait(barrier, line)
+
+    def info_copy(step):
+        peer = lax.rem(here + step, line)
+        return remote(
+            info_ref,
+            infos_ref.at[here],
+            info_send.at[step - 1],
+            info_recv.at[step - 1],
+            peer * 2 + side,
+        )
+
+    def row_copy(src, source, half, way):
+        unit = source * halves + half
+        return remote(
+            src,
+            held_ref.at[unit],
+            row_send.at[way, unit],
+            row_recv.at[unit],
+            place + (4 * way - 2),
+        )
+
+    def cross_copy(unit):
+        return remote(
+            cross_ref.at[unit],
+            crossed_ref.at[unit],
+            cross_send.at[unit],
+            cross_recv.at[unit],
+            twin,
+        )
+
+    def answer_copy(unit):
+        return remote(
+            answer_ref.at[unit],
+            done_ref.at[unit, pl.ds(slots, slots)],
+            answer_send.at[unit],
+            answer_recv.at[unit],
+            twin,
+        )
+
+    def sum_copy(target, half, way):
+        landing = (target + way) * halves + half
+        return remote(
+            part_ref.at[target * halves + half],
+            sum_ref.at[landing],
+            sum_send.at[target * halves + half],
+            sum_recv.at[landing],
+            place + (4 * way - 2),
+        )
+
+    for step in range(1, line):
+        info_copy(step).start()
+    for half in range(halves):
+        for way in range(2):
+
+            @pl.when((here < last) if way else (here > 0))
+            def _():
+                row_copy(rows_ref.at[half], here, half, way).start()
+
+    infos_ref[here] = info_ref[...]
+    for half in range(halves):
+        held_ref[here * halves + half] = rows_ref[half]
+    batch_ref[...] = jnp.zeros_like(batch_ref)
+    for step in range(1, line):
+        info_copy(step).wait()
+
+    shorter = jnp.minimum(here, last - here)
+
+    def source_of(k):
+        i = k // halves
+        paired = i <= 2 * shorter
+        near = (i + 1) // 2
+        near_source = here + near * (1 - 2 * lax.rem(i, 2))
+        far = i - shorter
+        far_source = jnp.where(here < last - here, here + far, here - far)
+        return jnp.where(paired, near_source, far_source), lax.rem(k, halves)
+
+    def matches(source, half, weighted):
+        info = infos_ref[source, half]
+        rank = lax.broadcasted_iota(jnp.int32, (slots, tokens), 0).astype(jnp.float32)
+        tables = []
+        for expert in (place, twin):
+            name = expert.astype(jnp.float32)
+            table = jnp.zeros((slots, tokens), jnp.float32)
+            for route in range(2):
+                hit = jnp.where(info[route : route + 1] == name, info[2 + route : 3 + route], -1.0)
+                value = info[4 + route : 5 + route] if weighted else 1.0
+                table += jnp.where(hit == rank, value, 0.0)
+            tables.append(table)
+        return jnp.concatenate(tables, axis=0)
+
+    def step_body(k, carry):
+        @pl.when(k < units)
+        def _():
+            source, half = source_of(k)
+            unit = source * halves + half
+
+            @pl.when(source != here)
+            def _():
+                remote(
+                    held_ref.at[unit], held_ref.at[unit], row_send.at[0, unit], row_recv.at[unit], twin
+                ).wait_recv()
+
+            @pl.when((source < here) & (here < last))
+            def _():
+                row_copy(held_ref.at[unit], source, half, 1).start()
+
+            @pl.when((source > here) & (here > 0))
+            def _():
+                row_copy(held_ref.at[unit], source, half, 0).start()
+
+            packed = jnp.dot(
+                matches(source, half, False).astype(jnp.bfloat16),
+                held_ref[unit],
+                preferred_element_type=jnp.float32,
+            ).astype(jnp.bfloat16)
+            cross_ref[unit] = packed[slots:]
+            cross_copy(unit).start()
+            batch_ref[0:slots, :] = packed[:slots]
+
+        @pl.when(k == 0)
+        def _():
+            for load in loads:
+                load.wait()
+
+        @pl.when((k > 0) & (k <= units))
+        def _():
+            source, half = source_of(k - 1)
+            unit = source * halves + half
+            cross_copy(unit).wait_recv()
+            batch_ref[slots : 2 * slots, :] = crossed_ref[unit]
+
+        @pl.when(k <= units)
+        def _():
+            rows = batch_ref[...]
+            gate = jnp.dot(rows, gate_ref[0], preferred_element_type=jnp.float32)
+            up = jnp.dot(rows, up_ref[0], preferred_element_type=jnp.float32)
+            active = (jax.nn.silu(gate) * up).astype(jnp.bfloat16)
+            batch_ref[...] = jnp.dot(
+                active, down_ref[0], preferred_element_type=jnp.float32
+            ).astype(jnp.bfloat16)
+
+        @pl.when(k < units)
+        def _():
+            source, half = source_of(k)
+            done_ref[source * halves + half, 0:slots, :] = batch_ref[0:slots, :]
+
+        @pl.when((k > 0) & (k <= units))
+        def _():
+            source, half = source_of(k - 1)
+            unit = source * halves + half
+            answer_ref[unit] = batch_ref[slots : 2 * slots, :]
+            answer_copy(unit).start()
+
+        @pl.when(k > 1)
+        def _():
+            source, half = source_of(k - 2)
+            unit = source * halves + half
+            answer_copy(unit).wait_recv()
+            high, low = split_two(matches(source, half, True))
+            answers = done_ref[unit]
+            turned = (((0,), (0,)), ((), ()))
+            part = lax.dot_general(
+                high, answers, turned, preferred_element_type=jnp.float32
+            ) + lax.dot_general(low, answers, turned, preferred_element_type=jnp.float32)
+
+            @pl.when(source == here)
+            def _():
+                own_ref[half] = part
+
+            @pl.when(source != here)
+            def _():
+                part_ref[unit] = part.astype(jnp.bfloat16)
+
+            @pl.when((source < here) & (here == last))
+            def _():
+                sum_copy(source, half, 0).start()
+
+            @pl.when((source > here) & (here == 0))
+            def _():
+                sum_copy(source, half, 1).start()
+
+        return carry
+
+    lax.fori_loop(0, units + 2, step_body, 0)
+
+    def relay(way):
+        for ahead in range(1, line):
+            target = here + ahead * (2 * way - 1)
+            for half in range(halves):
+
+                @pl.when((target >= 0) & (target <= last) & (here > 0) & (here < last))
+                def _():
+                    unit = target * halves + half
+                    landing = (target + way) * halves + half
+                    remote(
+                        part_ref.at[unit],
+                        sum_ref.at[landing],
+                        sum_send.at[unit],
+                        sum_recv.at[landing],
+                        twin,
+                    ).wait_recv()
+                    part_ref[unit] = (
+                        part_ref[unit].astype(jnp.float32) + sum_ref[landing].astype(jnp.float32)
+                    ).astype(jnp.bfloat16)
+                    sum_copy(target, half, way).start()
+
+    first_way = jnp.where(last - here <= here, 0, 1)
+    relay(first_way)
+    relay(1 - first_way)
+
+    for half in range(halves):
+        own_ref[half] = own_ref[half] + mix_ref[half]
+        for way in range(2):
+
+            @pl.when((here > 0) if way else (here < last))
+            def _():
+                landing = (here + way) * halves + half
+                remote(
+                    part_ref.at[0], sum_ref.at[landing], sum_send.at[0], sum_recv.at[landing], twin
+                ).wait_recv()
+                own_ref[half] = own_ref[half] + sum_ref[landing].astype(jnp.float32)
+
+        out_ref[half] = own_ref[half].astype(out_ref.dtype)
+
+    def drain(unit, carry):
+        source = unit // halves
+        half = lax.rem(unit, halves)
+        cross_copy(unit).wait_send()
+        answer_copy(unit).wait_send()
+
+        @pl.when((source <= here) & (here < last))
+        def _():
+            row_copy(held_ref.at[unit], source, half, 1).wait_send()
+
+        @pl.when((source >= here) & (here > 0))
+        def _():
+            row_copy(held_ref.at[unit], source, half, 0).wait_send()
+
+        @pl.when(source != here)
+        def _():
+            sum_copy(source, half, 0).wait_send()
+
+        return carry
+
+    lax.fori_loop(0, units, drain, 0)
+
+
+def run_line(normed_rows, after_mix, info, w_gate, w_up, w_down, slots):
+    count = lax.axis_size("sp")
+    line, halves = count // 2, info.shape[0]
+    units = line * halves
+    row_count, width = normed_rows.shape
+    tokens = row_count // halves
+    vmem = pl.BlockSpec(memory_space=pltpu.VMEM)
+    whole = pl.BlockSpec(memory_space=pl.ANY)
+    dma = pltpu.SemaphoreType.DMA
+    out = pl.pallas_call(
+        functools.partial(line_kernel, line=line, halves=halves, slots=slots),
+        out_shape=jax.ShapeDtypeStruct((halves, tokens, width), jnp.bfloat16),
+        in_specs=[vmem, vmem, vmem, whole, whole, whole],
+        out_specs=vmem,
+        scratch_shapes=[
+            pltpu.VMEM(w_gate.shape, jnp.bfloat16),
+            pltpu.VMEM(w_up.shape, jnp.bfloat16),
+            pltpu.VMEM(w_down.shape, jnp.bfloat16),
+            pltpu.VMEM((line,) + info.shape, jnp.float32),
+            pltpu.VMEM((units, tokens, width), jnp.bfloat16),
+            pltpu.VMEM((units, slots, width), jnp.bfloat16),
+            pltpu.VMEM((units, slots, width), jnp.bfloat16),
+            pltpu.VMEM((units, slots, width), jnp.bfloat16),
+            pltpu.VMEM((units, 2 * slots, width), jnp.bfloat16),
+            pltpu.VMEM((2 * slots, width), jnp.bfloat16),
+            pltpu.VMEM((units, tokens, width), jnp.bfloat16),
+            pltpu.VMEM((halves, tokens, width), jnp.float32),
+            pltpu.VMEM((units + halves, tokens, width), jnp.bfloat16),
+            dma((3,)),
+            dma((line - 1,)),
+            dma((line - 1,)),
+            dma((2, units)),
+            dma((units,)),
+            dma((units,)),
+            dma((units,)),
+            dma((units,)),
+            dma((units,)),
+            dma((units,)),
+            dma((units + halves,)),
+        ],
+        compiler_params=pltpu.CompilerParams(
+            vmem_limit_bytes=VMEM_LIMIT, collective_id=4, has_side_effects=True
+        ),
+        cost_estimate=pl.CostEstimate(flops=10**10, bytes_accessed=2**23, transcendentals=0),
+        name="experts",
+    )(
+        normed_rows.reshape(halves, tokens, width),
+        after_mix.reshape(halves, tokens, width),
+        info,
+        w_gate,
+        w_up,
+        w_down,
+    )
+    return out.reshape(row_count, width)
+
+
+def route_info(routes, route_weight, halves):
+    tokens = routes.shape[0] // halves
+    ids = routes.reshape(halves, -1)
+    order = jnp.arange(ids.shape[1], dtype=jnp.int32)
+    same = (ids[:, :, None] == ids[:, None, :]) & (order[None, None, :] < order[None, :, None])
+    rank = jnp.sum(same.astype(jnp.float32), axis=2)
+
+    def turned(a):
+        return a.astype(jnp.float32).reshape(halves, tokens, -1).transpose(0, 2, 1)
+
+    return jnp.concatenate(
+        [turned(routes), turned(rank), turned(route_weight), jnp.zeros((halves, 2, tokens), jnp.float32)],
+        axis=1,
+    )
+
+
 def shards(
     resid,
     query,
@@ -544,6 +939,10 @@
         * lax.rsqrt(jnp.mean(after_mix * after_mix, axis=1, keepdims=True) + EPS)
         * ffn_gain[None, :]
     ).astype(jnp.bfloat16)
+    dense = local_experts == 1 and sources % 2 == 0 and route_count == 2
+    if dense and 2 * capacity >= half_rows and capacity % 16 == 0:
+        info = route_info(routes, route_weight, 2)
+        return run_line(normed_rows, after_mix, info, w_gate, w_up, w_down, capacity)
     selects = [
         slot_select(
             routes[half_idx * half_rows : (half_idx + 1) * half_rows], expert_count, capacity

time: 209 us -> 164 us (0.78)
  the two profiles are of different devices: /device:TPU:13 before, /device:TPU:0 now
where the time goes in v2:
time: 164 us
  Pallas kernels  152 us (93%)
  other arithmetic  5.46 us (3%)
  local copies, waits for them, and re-layouts  3.64 us (2%)
  matrix products  2.29 us (1%)
    pallas_call x1, Pallas kernels, run_line(): pl.pallas_call(functools.partial(line_kernel, line=line, halves=halves, s...  125 us
    pallas_call x1, Pallas kernels, run_cell_scan(): pl.pallas_call(functools.partial(cell_kernel, count=count, heads=heads, t...  27.4 us

profile of v2, /device:TPU:0, one launch (start us, length us, event | category | flops | bytes accessed | tf_op | source)
XLA Modules:
  0.0 163.7 jit_solution(10677757244996883007)
XLA Ops:
  0.0 0.1 pad.3.clone
  0.1 0.7 reduce_sum.39
  0.8 0.7 broadcast_divide_fusion
  1.5 0.1 reshape.58
  1.6 0.7 convert_element_type.26
  2.2 0.1 reshape.56
  2.4 0.8 copy.21
  3.2 0.1 eq.15
  3.3 0.3 convert_reduce_fusion
  3.6 0.1 reshape.57
  3.7 0.1 copy.22
  3.8 0.7 maximum_maximum_fusion.info_ref
  4.5 0.0 copy-start.2
  4.5 0.0 copy-start.3
  4.5 0.0 copy-start.4
  4.5 0.0 copy-start.5
  4.5 27.4 %cell.1 = bf16[192,1024]{1,0:T(8,128)(2,1)} custom-call(bf16[768,256]{1,0:T(8,128)(2,1)} %q_ref.1, bf16[768,256]{1,0:T(8,128)(2,1)} %k_ref.1, bf16[768,256]{1,0:T(8,128)(2,1)} %v_ref.1, f32[1,768]{1,0:T(1,128)} %forget_ref.1, f32[1,768]{1,0:T(1,128)} %input_ref.1), custom_call_target="tpu_custom_call" | custom-call | flops 10000000000 | bytes 2097152 | tf_op jit(solution)/shard_map/cell/pallas_call | solution.py:395
  31.9 1.2 fusion
  33.0 0.0 copy-done.2
  33.0 0.0 copy-done.3
  33.0 0.0 copy-done.4
  33.0 0.0 copy-done.5
  33.1 0.0 copy-start.1
  33.1 2.3 %multiply_reduce_fusion = (f32[192]{0:T(256)S(1)}, f32[192,2048]{1,0:T(8,128)S(1)}) fusion(bf16[1024,2048]{1,0:T(8,128)(2,1)S(1)} %copy-done.2, bf16[192,1024]{1,0:T(8,128)(2,1)} %cell.1, bf16[192,1024]{1,0:T(8,128)(2,1)S(1)} %copy-done.4, f32[1024]{0:T(1024)S(1)} %copy-done.5, f32[192]{0:T(256)S(1)} %add_rsqrt_fusion.1, bf16[192,2048]{1,0:T(8,128)(2,1)S(1)} %copy-done.3), kind=kOutput, calls=%fused_computation.2 | convolution fusion | flops 808648512 | bytes 7345664 | tf_op jit(solution)/shard_map/dot_general | solution.py:934
  35.4 0.0 copy-start
  35.4 0.0 copy-done.1
  35.4 1.3 multiply_convert_fusion
  36.7 0.1 copy-done
  36.8 124.8 %experts.1 = bf16[2,96,2048]{2,1,0:T(8,128)(2,1)} custom-call(bf16[2,96,2048]{2,1,0:T(8,128)(2,1)} %bitcast.15, f32[2,96,2048]{2,1,0:T(8,128)} %bitcast.13, f32[2,8,96]{2,1,0:T(8,128)} %maximum_maximum_fusion.info_ref, bf16[1,2048,512]{2,1,0:T(8,128)(2,1)} %gate_hbm.1, bf16[1,2048,512]{2,1,0:T(8,128)(2,1)} %up_hbm.1, bf16[1,512,2048]{2,1,0:T(8,128)(2,1)} %down_hbm.1), custom_call_target="tpu_custom_call" | custom-call | flops 10000000000 | bytes 8388608 | tf_op jit(solution)/shard_map/experts/pallas_call | solution.py:838
  161.6 2.1 %copy.27 = bf16[192,2048]{1,0:T(8,128)(2,1)} copy(bf16[192,2048]{1,0:T(8,128)(2,1)} %bitcast.14) | data formatting | bytes 1572864
  (5 shorter events, 0.0 us)
Async XLA Ops:
  4.5 28.6 %copy-start.2 = (bf16[1024,2048]{1,0:T(8,128)(2,1)S(1)}, bf16[1024,2048]{1,0:T(8,128)(2,1)}, u32[]{:S(2)}) copy-start(bf16[1024,2048]{1,0:T(8,128)(2,1)} %param.23) | copy-start | bytes 12582916
  4.5 28.6 %copy-start.3 = (bf16[192,2048]{1,0:T(8,128)(2,1)S(1)}, bf16[192,2048]{1,0:T(8,128)(2,1)}, u32[]{:S(2)}) copy-start(bf16[192,2048]{1,0:T(8,128)(2,1)} %param.15) | copy-start | bytes 2359300
  4.5 28.6 %copy-start.4 = (bf16[192,1024]{1,0:T(8,128)(2,1)S(1)}, bf16[192,1024]{1,0:T(8,128)(2,1)}, u32[]{:S(2)}) copy-start(bf16[192,1024]{1,0:T(8,128)(2,1)} %param.19) | copy-start | bytes 1179652
  4.5 28.6 %copy-start.5 = (f32[1024]{0:T(1024)S(1)}, f32[1024]{0:T(1024)}, u32[]{:S(2)}) copy-start(f32[1024]{0:T(1024)} %param.22) | copy-start | bytes 12292
  33.1 2.3 %copy-start.1 = (f32[2048]{0:T(1024)S(1)}, f32[2048]{0:T(1024)}, u32[]{:S(2)}) copy-start(f32[2048]{0:T(1024)} %param.24) | copy-start | bytes 24580
  35.4 1.4 copy-start

commit v3 on v2

--- a/solution.py
+++ b/solution.py
@@ -539,6 +539,7 @@
     line,
     halves,
     slots,
+    pieces,
 ):
     place = lax.axis_index("sp")
     here = place // 2
@@ -546,6 +547,7 @@
     twin = place + 1 - 2 * side
     units = line * halves
     tokens = rows_ref.shape[1]
+    grain = tokens // pieces
     last = line - 1
 
     def remote(src, dst, send, recv, peer):
@@ -618,24 +620,41 @@
             twin,
         )
 
-    def sum_copy(target, half, way):
-        landing = (target + way) * halves + half
+    def sum_copy(target, half, way, piece):
+        landing = ((target + way) * halves + half) * pieces + piece
+        leaving = (target * halves + half) * pieces + piece
         return remote(
-            part_ref.at[target * halves + half],
+            part_ref.at[leaving],
             sum_ref.at[landing],
-            sum_send.at[target * halves + half],
+            sum_send.at[leaving],
             sum_recv.at[landing],
             place + (4 * way - 2),
         )
 
+    def sum_wait(landing):
+        remote(
+            part_ref.at[0], sum_ref.at[landing], sum_send.at[0], sum_recv.at[landing], twin
+        ).wait_recv()
+
     for step in range(1, line):
         info_copy(step).start()
-    for half in range(halves):
-        for way in range(2):
-
-            @pl.when((here < last) if way else (here > 0))
-            def _():
-                row_copy(rows_ref.at[half], here, half, way).start()
+    for way in range(2):
+
+        @pl.when((here < last) if way else (here > 0))
+        def _():
+            row_copy(rows_ref.at[0], here, 0, way).start()
+
+    def later_halves(way):
+        for half in range(1, halves):
+            row_copy(rows_ref.at[half], here, half, way).start()
+
+    @pl.when(here == 0)
+    def _():
+        later_halves(1)
+
+    @pl.when(here == last)
+    def _():
+        later_halves(0)
 
     infos_ref[here] = info_ref[...]
     for half in range(halves):
@@ -646,14 +665,27 @@
 
     shorter = jnp.minimum(here, last - here)
 
+    def in_stream(p, reach):
+        first = p < reach
+        turn = p - reach
+        ahead = jnp.where(first, p + 1, reach - turn // (halves - 1))
+        return ahead, jnp.where(first, 0, 1 + lax.rem(turn, halves - 1))
+
     def source_of(k):
-        i = k // halves
-        paired = i <= 2 * shorter
-        near = (i + 1) // 2
-        near_source = here + near * (1 - 2 * lax.rem(i, 2))
-        far = i - shorter
-        far_source = jnp.where(here < last - here, here + far, here - far)
-        return jnp.where(paired, near_source, far_source), lax.rem(k, halves)
+        p = k - halves
+        both = shorter * 2 * halves
+        paired = p < both
+        way = jnp.where(paired, lax.rem(p, 2), jnp.where(here < last - here, 1, 0))
+        spot = jnp.where(paired, p // 2, p - shorter * halves)
+        reach = jnp.where(way == 1, last - here, here)
+        ahead, half = in_stream(spot, reach)
+        is_own = k < halves
+        final = spot == reach * halves - 1
+        return (
+            jnp.where(is_own, here, here + ahead * (2 * way - 1)),
+            jnp.where(is_own, k, half),
+            final,
+        )
 
     def matches(source, half, weighted):
         info = infos_ref[source, half]
@@ -669,10 +701,28 @@
             tables.append(table)
         return jnp.concatenate(tables, axis=0)
 
+    first_way = jnp.where(last - here <= here, 0, 1)
+
+    def relay(way, spot):
+        reach = jnp.where(way == 1, last - here, here)
+
+        @pl.when((spot >= 0) & (spot < reach * halves) & (here > 0) & (here < last))
+        def _():
+            ahead, half = in_stream(spot, reach)
+            target = here + ahead * (2 * way - 1)
+            for piece in range(pieces):
+                unit = (target * halves + half) * pieces + piece
+                landing = ((target + way) * halves + half) * pieces + piece
+                sum_wait(landing)
+                part_ref[unit] = (
+                    part_ref[unit].astype(jnp.float32) + sum_ref[landing].astype(jnp.float32)
+                ).astype(jnp.bfloat16)
+                sum_copy(target, half, way, piece).start()
+
     def step_body(k, carry):
         @pl.when(k < units)
         def _():
-            source, half = source_of(k)
+            source, half, final = source_of(k)
             unit = source * halves + half
 
             @pl.when(source != here)
@@ -685,9 +735,17 @@
             def _():
                 row_copy(held_ref.at[unit], source, half, 1).start()
 
+                @pl.when(final)
+                def _():
+                    later_halves(1)
+
             @pl.when((source > here) & (here > 0))
             def _():
                 row_copy(held_ref.at[unit], source, half, 0).start()
+
+                @pl.when(final)
+                def _():
+                    later_halves(0)
 
             packed = jnp.dot(
                 matches(source, half, False).astype(jnp.bfloat16),
@@ -703,9 +761,11 @@
             for load in loads:
                 load.wait()
 
+        relay(first_way, k - units)
+
         @pl.when((k > 0) & (k <= units))
         def _():
-            source, half = source_of(k - 1)
+            source, half, _ = source_of(k - 1)
             unit = source * halves + half
             cross_copy(unit).wait_recv()
             batch_ref[slots : 2 * slots, :] = crossed_ref[unit]
@@ -722,19 +782,29 @@
 
         @pl.when(k < units)
         def _():
-            source, half = source_of(k)
+            source, half, _ = source_of(k)
             done_ref[source * halves + half, 0:slots, :] = batch_ref[0:slots, :]
 
         @pl.when((k > 0) & (k <= units))
         def _():
-            source, half = source_of(k - 1)
+            source, half, _ = source_of(k - 1)
             unit = source * halves + half
             answer_ref[unit] = batch_ref[slots : 2 * slots, :]
-            answer_copy(unit).start()
-
-        @pl.when(k > 1)
-        def _():
-            source, half = source_of(k - 2)
+
+            @pl.when(source != here)
+            def _():
+                answer_copy(unit).start()
+
+        @pl.when(k == units)
+        def _():
+            for half in range(halves):
+                answer_copy(here * halves + half).start()
+
+        relay(1 - first_way, k - units - 2)
+
+        @pl.when(k > 1 + halves)
+        def _():
+            source, half, _ = source_of(jnp.where(k > units + 1, k - units - 2, k - 2))
             unit = source * halves + half
             answer_copy(unit).wait_recv()
             high, low = split_two(matches(source, half, True))
@@ -750,58 +820,38 @@
 
             @pl.when(source != here)
             def _():
-                part_ref[unit] = part.astype(jnp.bfloat16)
+                for piece in range(pieces):
+                    part_ref[unit * pieces + piece] = part[
+                        piece * grain : (piece + 1) * grain
+                    ].astype(jnp.bfloat16)
 
             @pl.when((source < here) & (here == last))
             def _():
-                sum_copy(source, half, 0).start()
+                for piece in range(pieces):
+                    sum_copy(source, half, 0, piece).start()
 
             @pl.when((source > here) & (here == 0))
             def _():
-                sum_copy(source, half, 1).start()
+                for piece in range(pieces):
+                    sum_copy(source, half, 1, piece).start()
 
         return carry
 
-    lax.fori_loop(0, units + 2, step_body, 0)
-
-    def relay(way):
-        for ahead in range(1, line):
-            target = here + ahead * (2 * way - 1)
-            for half in range(halves):
-
-                @pl.when((target >= 0) & (target <= last) & (here > 0) & (here < last))
+    lax.fori_loop(0, units + 2 + halves, step_body, 0)
+
+    for half in range(halves):
+        for piece in range(pieces):
+            rows = pl.ds(piece * grain, grain)
+            own_ref[half, rows] = own_ref[half, rows] + mix_ref[half, rows]
+            for way in range(2):
+
+                @pl.when((here > 0) if way else (here < last))
                 def _():
-                    unit = target * halves + half
-                    landing = (target + way) * halves + half
-                    remote(
-                        part_ref.at[unit],
-                        sum_ref.at[landing],
-                        sum_send.at[unit],
-                        sum_recv.at[landing],
-                        twin,
-                    ).wait_recv()
-                    part_ref[unit] = (
-                        part_ref[unit].astype(jnp.float32) + sum_ref[landing].astype(jnp.float32)
-                    ).astype(jnp.bfloat16)
-                    sum_copy(target, half, way).start()
-
-    first_way = jnp.where(last - here <= here, 0, 1)
-    relay(first_way)
-    relay(1 - first_way)
-
-    for half in range(halves):
-        own_ref[half] = own_ref[half] + mix_ref[half]
-        for way in range(2):
-
-            @pl.when((here > 0) if way else (here < last))
-            def _():
-                landing = (here + way) * halves + half
-                remote(
-                    part_ref.at[0], sum_ref.at[landing], sum_send.at[0], sum_recv.at[landing], twin
-                ).wait_recv()
-                own_ref[half] = own_ref[half] + sum_ref[landing].astype(jnp.float32)
-
-        out_ref[half] = own_ref[half].astype(out_ref.dtype)
+                    landing = ((here + way) * halves + half) * pieces + piece
+                    sum_wait(landing)
+                    own_ref[half, rows] = own_ref[half, rows] + sum_ref[landing].astype(jnp.float32)
+
+            out_ref[half, rows] = own_ref[half, rows].astype(out_ref.dtype)
 
     def drain(unit, carry):
         source = unit // halves
@@ -819,7 +869,8 @@
 
         @pl.when(source != here)
         def _():
-            sum_copy(source, half, 0).wait_send()
+            for piece in range(pieces):
+                sum_copy(source, half, 0, piece).wait_send()
 
         return carry
 
@@ -832,11 +883,13 @@
     units = line * halves
     row_count, width = normed_rows.shape
     tokens = row_count // halves
+    pieces = 2
+    grain = tokens // pieces
     vmem = pl.BlockSpec(memory_space=pltpu.VMEM)
     whole = pl.BlockSpec(memory_space=pl.ANY)
     dma = pltpu.SemaphoreType.DMA
     out = pl.pallas_call(
-        functools.partial(line_kernel, line=line, halves=halves, slots=slots),
+        functools.partial(line_kernel, line=line, halves=halves, slots=slots, pieces=pieces),
         out_shape=jax.ShapeDtypeStruct((halves, tokens, width), jnp.bfloat16),
         in_specs=[vmem, vmem, vmem, whole, whole, whole],
         out_specs=vmem,
@@ -851,9 +904,9 @@
             pltpu.VMEM((units, slots, width), jnp.bfloat16),
             pltpu.VMEM((units, 2 * slots, width), jnp.bfloat16),
             pltpu.VMEM((2 * slots, width), jnp.bfloat16),
-            pltpu.VMEM((units, tokens, width), jnp.bfloat16),
+            pltpu.VMEM((units * pieces, grain, width), jnp.bfloat16),
             pltpu.VMEM((halves, tokens, width), jnp.float32),
-            pltpu.VMEM((units + halves, tokens, width), jnp.bfloat16),
+            pltpu.VMEM(((units + halves) * pieces, grain, width), jnp.bfloat16),
             dma((3,)),
             dma((line - 1,)),
             dma((line - 1,)),
@@ -863,8 +916,8 @@
             dma((units,)),
             dma((units,)),
             dma((units,)),
-            dma((units,)),
-            dma((units + halves,)),
+            dma((units * pieces,)),
+            dma(((units + halves) * pieces,)),
         ],
         compiler_params=pltpu.CompilerParams(
             vmem_limit_bytes=VMEM_LIMIT, collective_id=4, has_side_effects=True
@@ -939,8 +992,8 @@
         * lax.rsqrt(jnp.mean(after_mix * after_mix, axis=1, keepdims=True) + EPS)
         * ffn_gain[None, :]
     ).astype(jnp.bfloat16)
-    dense = local_experts == 1 and sources % 2 == 0 and route_count == 2
-    if dense and 2 * capacity >= half_rows and capacity % 16 == 0:
+    dense = local_experts == 1 and sources % 2 == 0 and sources <= 8 and route_count == 2
+    if dense and 2 * capacity >= half_rows and capacity % 16 == 0 and half_rows % 32 == 0:
         info = route_info(routes, route_weight, 2)
         return run_line(normed_rows, after_mix, info, w_gate, w_up, w_down, capacity)
     selects = [

time: 164 us -> 139 us (0.85)
  Pallas kernels: 152 us -> 127 us
    pallas_call x1, Pallas kernels: 125 us -> 100 us  [run_line(): pl.pallas_call(functools.partial(line_kernel, line=line, halves=halves, s...]
where the time goes in v3:
time: 139 us
  Pallas kernels  127 us (91%)
  other arithmetic  5.46 us (4%)
  local copies, waits for them, and re-layouts  3.64 us (3%)
  matrix products  2.29 us (2%)
    pallas_call x1, Pallas kernels, run_line(): pl.pallas_call(functools.partial(line_kernel, line=line, halves=halves, s...  100 us
    pallas_call x1, Pallas kernels, run_cell_scan(): pl.pallas_call(functools.partial(cell_kernel, count=count, heads=heads, t...  27.4 us
    unnamed x14, local copies, waits for them, and re-layouts  3.03 us

profile of v3, /device:TPU:0, one launch (start us, length us, event | category | flops | bytes accessed | tf_op | source)
XLA Modules:
  0.0 139.0 jit_solution(17348245041766701045)
XLA Ops:
  0.0 0.1 pad.3.clone
  0.1 0.7 reduce_sum.39
  0.8 0.7 broadcast_divide_fusion
  1.5 0.1 reshape.58
  1.6 0.7 convert_element_type.26
  2.2 0.1 reshape.56
  2.4 0.8 copy.21
  3.2 0.1 eq.15
  3.3 0.3 convert_reduce_fusion
  3.6 0.1 reshape.57
  3.7 0.1 copy.22
  3.8 0.7 maximum_maximum_fusion.info_ref
  4.5 0.0 copy-start.2
  4.5 0.0 copy-start.3
  4.5 0.0 copy-start.4
  4.5 0.0 copy-start.5
  4.5 27.4 %cell.1 = bf16[192,1024]{1,0:T(8,128)(2,1)} custom-call(bf16[768,256]{1,0:T(8,128)(2,1)} %q_ref.1, bf16[768,256]{1,0:T(8,128)(2,1)} %k_ref.1, bf16[768,256]{1,0:T(8,128)(2,1)} %v_ref.1, f32[1,768]{1,0:T(1,128)} %forget_ref.1, f32[1,768]{1,0:T(1,128)} %input_ref.1), custom_call_target="tpu_custom_call" | custom-call | flops 10000000000 | bytes 2097152 | tf_op jit(solution)/shard_map/cell/pallas_call | solution.py:395
  31.9 1.2 fusion
  33.0 0.0 copy-done.2
  33.0 0.0 copy-done.3
  33.0 0.0 copy-done.4
  33.0 0.0 copy-done.5
  33.1 0.0 copy-start.1
  33.1 2.3 %multiply_reduce_fusion = (f32[192]{0:T(256)S(1)}, f32[192,2048]{1,0:T(8,128)S(1)}) fusion(bf16[1024,2048]{1,0:T(8,128)(2,1)S(1)} %copy-done.2, bf16[192,1024]{1,0:T(8,128)(2,1)} %cell.1, bf16[192,1024]{1,0:T(8,128)(2,1)S(1)} %copy-done.4, f32[1024]{0:T(1024)S(1)} %copy-done.5, f32[192]{0:T(256)S(1)} %add_rsqrt_fusion.1, bf16[192,2048]{1,0:T(8,128)(2,1)S(1)} %copy-done.3), kind=kOutput, calls=%fused_computation.2 | convolution fusion | flops 808648512 | bytes 7345664 | tf_op jit(solution)/shard_map/dot_general | solution.py:987
  35.4 0.0 copy-start
  35.4 0.0 copy-done.1
  35.4 1.3 multiply_convert_fusion
  36.7 0.1 copy-done
  36.8 100.1 %experts.1 = bf16[2,96,2048]{2,1,0:T(8,128)(2,1)} custom-call(bf16[2,96,2048]{2,1,0:T(8,128)(2,1)} %bitcast.15, f32[2,96,2048]{2,1,0:T(8,128)} %bitcast.13, f32[2,8,96]{2,1,0:T(8,128)} %maximum_maximum_fusion.info_ref, bf16[1,2048,512]{2,1,0:T(8,128)(2,1)} %gate_hbm.1, bf16[1,2048,512]{2,1,0:T(8,128)(2,1)} %up_hbm.1, bf16[1,512,2048]{2,1,0:T(8,128)(2,1)} %down_hbm.1), custom_call_target="tpu_custom_call" | custom-call | flops 10000000000 | bytes 8388608 | tf_op jit(solution)/shard_map/experts/pallas_call | solution.py:891
  136.9 2.1 %copy.27 = bf16[192,2048]{1,0:T(8,128)(2,1)} copy(bf16[192,2048]{1,0:T(8,128)(2,1)} %bitcast.14) | data formatting | bytes 1572864
  (5 shorter events, 0.0 us)
Async XLA Ops:
  4.5 28.6 %copy-start.2 = (bf16[1024,2048]{1,0:T(8,128)(2,1)S(1)}, bf16[1024,2048]{1,0:T(8,128)(2,1)}, u32[]{:S(2)}) copy-start(bf16[1024,2048]{1,0:T(8,128)(2,1)} %param.23) | copy-start | bytes 12582916
  4.5 28.6 %copy-start.3 = (bf16[192,2048]{1,0:T(8,128)(2,1)S(1)}, bf16[192,2048]{1,0:T(8,128)(2,1)}, u32[]{:S(2)}) copy-start(bf16[192,2048]{1,0:T(8,128)(2,1)} %param.15) | copy-start | bytes 2359300
  4.5 28.6 %copy-start.4 = (bf16[192,1024]{1,0:T(8,128)(2,1)S(1)}, bf16[192,1024]{1,0:T(8,128)(2,1)}, u32[]{:S(2)}) copy-start(bf16[192,1024]{1,0:T(8,128)(2,1)} %param.19) | copy-start | bytes 1179652
  4.5 28.6 %copy-start.5 = (f32[1024]{0:T(1024)S(1)}, f32[1024]{0:T(1024)}, u32[]{:S(2)}) copy-start(f32[1024]{0:T(1024)} %param.22) | copy-start | bytes 12292
  33.1 2.3 %copy-start.1 = (f32[2048]{0:T(1024)S(1)}, f32[2048]{0:T(1024)}, u32[]{:S(2)}) copy-start(f32[2048]{0:T(1024)} %param.24) | copy-start | bytes 24580
  35.4 1.4 %copy-start = (f32[192,2048]{1,0:T(8,128)}, f32[192,2048]{1,0:T(8,128)S(1)}, u32[]{:S(2)}) copy-start(f32[192,2048]{1,0:T(8,128)S(1)} %get-tuple-element.6) | copy-start | bytes 4718596

commit v4 on v3

--- a/solution.py
+++ b/solution.py
@@ -17,6 +17,8 @@
 
 EXTRA = 8
 VMEM_LIMIT = 56 * 1024 * 1024
+LAYER_VMEM = 60 * 1024 * 1024
+WEIGHT_PIECES = 4
 
 
 def col_mask(first_row, rows, cols):
@@ -429,6 +431,766 @@
         return run_cell_scan(query, keys, values, forget_pre, input_pre)
     rows = run_cell(query, keys, values, forget_pre, input_pre)
     return lax.all_to_all(rows, "tp", split_axis=0, concat_axis=1, tiled=True)
+
+
+def layer_kernel(
+    q_ref,
+    k_ref,
+    v_ref,
+    forget_ref,
+    input_ref,
+    head_gain_ref,
+    ffn_gain_ref,
+    routes_ref,
+    scores_ref,
+    resid_hbm,
+    out_gate_hbm,
+    out_proj_hbm,
+    gate_hbm,
+    up_hbm,
+    down_hbm,
+    out_ref,
+    state_ref,
+    piece_ref,
+    extra_ref,
+    prefix_ref,
+    mat_ref,
+    num_ref,
+    aux_ref,
+    cell_ref,
+    token_ref,
+    resid_ref,
+    out_gate_ref,
+    out_proj_ref,
+    gate_ref,
+    up_ref,
+    down_ref,
+    twin_gate_ref,
+    twin_up_ref,
+    twin_down_ref,
+    infos_ref,
+    rows_ref,
+    held_ref,
+    cross_ref,
+    done_ref,
+    part_ref,
+    own_ref,
+    sum_ref,
+    load_sems,
+    own_sem,
+    send_sems,
+    recv_sems,
+    extra_send_sems,
+    extra_recv_sems,
+    back_send_sems,
+    back_recv_sems,
+    turn_send_sems,
+    turn_recv_sems,
+    info_send,
+    info_recv,
+    row_send,
+    row_recv,
+    sum_send,
+    sum_recv,
+    weight_send,
+    weight_recv,
+    *,
+    count,
+    heads,
+    line,
+    halves,
+    slots,
+    pieces,
+    tile,
+):
+    seq_len, width = q_ref.shape
+    cut = width // count
+    place = lax.axis_index("sp")
+    head = lax.axis_index("tp")
+    here = place // 2
+    side = lax.rem(place, 2)
+    twin = place + 1 - 2 * side
+    mate = head + 1 - 2 * lax.rem(head, 2)
+    across = lax.rem(head + 2, heads)
+    units = line * halves
+    tokens = rows_ref.shape[1]
+    grain = tokens // pieces
+    last = line - 1
+    shares = WEIGHT_PIECES
+    chunks = 3 * shares
+
+    def remote(src, dst, send, recv, peer, axis="sp"):
+        return pltpu.make_async_remote_copy(
+            src_ref=src,
+            dst_ref=dst,
+            send_sem=send,
+            recv_sem=recv,
+            device_id={axis: peer},
+            device_id_type=pl.DeviceIdType.MESH,
+        )
+
+    loads = [
+        pltpu.make_async_copy(src, dst, load_sems.at[i])
+        for i, (src, dst) in enumerate(
+            [
+                (out_gate_hbm, out_gate_ref),
+                (resid_hbm, resid_ref),
+                (out_proj_hbm, out_proj_ref),
+                (gate_hbm, gate_ref),
+                (up_hbm, up_ref),
+                (down_hbm, down_ref),
+            ]
+        )
+    ]
+    for load in loads:
+        load.start()
+
+    barrier = pltpu.get_barrier_semaphore()
+    greeted = sp_tp_barrier(barrier, {"sp": count, "tp": heads})
+
+    def weight_rows(chunk, owner):
+        source = (gate_hbm, up_hbm, down_hbm)[chunk // shares]
+        target = (twin_gate_ref, twin_up_ref, twin_down_ref)[chunk // shares]
+        quarter = target.shape[0] // heads
+        size = quarter // shares
+        start = owner * quarter + (chunk % shares) * size
+        rows = pl.ds(pl.multiple_of(start, size), size)
+        return source.at[0, rows], target.at[rows]
+
+    def weight_copy(stage, chunk):
+        owner, peer, axis = (
+            (head, twin, "sp"),
+            (head, across, "tp"),
+            (head, mate, "tp"),
+            (across, mate, "tp"),
+        )[stage]
+        whole, landed = weight_rows(chunk, owner)
+        return remote(
+            whole if stage == 0 else landed,
+            landed,
+            weight_send.at[stage, chunk],
+            weight_recv.at[stage, chunk],
+            peer,
+            axis,
+        )
+
+    def fetch(*span):
+        for chunk in range(*span):
+            weight_copy(0, chunk).start()
+
+    def pass_on(*span):
+        for chunk in range(*span):
+            weight_copy(0, chunk).wait_recv()
+            weight_copy(1, chunk).start()
+            weight_copy(2, chunk).start()
+
+    def hand_over(*span):
+        for chunk in range(*span):
+            weight_copy(1, chunk).wait_recv()
+            weight_copy(3, chunk).start()
+
+    def info_copy(step):
+        peer = lax.rem(here + step, line)
+        return remote(
+            infos_ref.at[here],
+            infos_ref.at[here],
+            info_send.at[step - 1],
+            info_recv.at[step - 1],
+            peer * 2 + side,
+        )
+
+    eye_row, eye_col = col_mask(0, tokens, tokens)
+    eye = jnp.where(eye_row == eye_col, 1.0, 0.0)
+    for half in range(halves):
+        span = slice(half * tokens, (half + 1) * tokens)
+        ids = routes_ref[:, span].astype(jnp.float32)
+        scores = scores_ref[:, span]
+        zeros = jnp.zeros((8 - ids.shape[0], tokens), jnp.float32)
+        columns = lax.dot_general(
+            eye,
+            jnp.concatenate([ids, zeros], axis=0),
+            (((1,), (1,)), ((), ())),
+            precision=HIGHEST,
+            preferred_element_type=jnp.float32,
+        )
+        ranks = []
+        for route in range(2):
+            rank = jnp.zeros((1, tokens), jnp.float32)
+            for other in range(2):
+                same = (columns[:, other : other + 1] == ids[route : route + 1]) & (eye_row < eye_col)
+                rank += jnp.sum(jnp.where(same, 1.0, 0.0), axis=0, keepdims=True)
+            ranks.append(rank)
+        infos_ref[here, half] = jnp.concatenate(
+            [ids] + ranks + [scores / jnp.sum(scores, axis=0, keepdims=True), zeros[0:2]], axis=0
+        )
+
+    log_forget, cum_row, gap_row = log_rows(forget_ref, input_ref)
+    pl.semaphore_wait(barrier, greeted)
+    fetch(0, 2)
+    total = jnp.sum(log_forget, axis=1, keepdims=True)
+    best = jnp.max(gap_row, axis=1, keepdims=True)
+    keep_row = jnp.exp(gap_row - best) * width ** (-0.5)
+    weighted = k_ref[...].astype(jnp.float32).T * keep_row
+    high, low = split_two(weighted)
+    v_all = v_ref[...]
+    state_ref[0:width, :] = jnp.dot(high, v_all, preferred_element_type=jnp.float32) + jnp.dot(
+        low, v_all, preferred_element_type=jnp.float32
+    )
+    vector = jnp.dot(
+        jnp.broadcast_to(keep_row, (8, seq_len)),
+        k_ref[...].astype(jnp.float32),
+        precision=HIGHEST,
+        preferred_element_type=jnp.float32,
+    )[0:1]
+    lanes = jnp.zeros((1, width), jnp.float32)
+    state_ref[width : width + EXTRA, :] = jnp.concatenate(
+        [vector, lanes + total, lanes + total + best, jnp.zeros((EXTRA - 3, width), jnp.float32)],
+        axis=0,
+    )
+    for step in range(1, line):
+        info_copy(step).start()
+    sends = []
+    for step in range(1, count):
+        peer = lax.rem(place + step, count)
+        extra_copy = pltpu.make_async_remote_copy(
+            src_ref=state_ref.at[pl.ds(width, EXTRA)],
+            dst_ref=extra_ref.at[place],
+            send_sem=extra_send_sems.at[step - 1],
+            recv_sem=extra_recv_sems.at[step - 1],
+            device_id={"sp": peer},
+            device_id_type=pl.DeviceIdType.MESH,
+        )
+        piece_copy = pltpu.make_async_remote_copy(
+            src_ref=state_ref.at[pl.ds(pl.multiple_of(peer * cut, cut), cut)],
+            dst_ref=piece_ref.at[place],
+            send_sem=send_sems.at[step - 1],
+            recv_sem=recv_sems.at[step - 1],
+            device_id={"sp": peer},
+            device_id_type=pl.DeviceIdType.MESH,
+        )
+        extra_copy.start()
+        piece_copy.start()
+        sends += [extra_copy, piece_copy]
+    extra_ref[place] = state_ref[width : width + EXTRA, :]
+    piece_ref[place] = state_ref[pl.ds(pl.multiple_of(place * cut, cut), cut), :]
+
+    fetch(2, 4)
+
+    for first in range(0, seq_len, tile):
+        span = first + tile
+        row, col = col_mask(first, tile, span)
+        causal = col <= row
+        own = (col // BLOCK) == (row // BLOCK)
+        gap = jnp.where(causal, gap_row[:, :span], -jnp.inf)
+        top = jnp.max(gap, axis=1, keepdims=True)
+        cum = jnp.sum(jnp.where(causal, log_forget[:, :span], 0.0), axis=1, keepdims=True)
+        scores = lax.dot_general(
+            q_ref[first:span, :],
+            k_ref[0:span, :],
+            (((1,), (1,)), ((), ())),
+            preferred_element_type=jnp.float32,
+        ) * width ** (-0.5)
+        weights = scores * jnp.exp(gap - top)
+        high = weights.astype(jnp.bfloat16)
+        high_float = high.astype(jnp.float32)
+        low_float = jnp.where(own, 0.0, weights - high_float)
+        v = v_ref[0:span, :]
+        num_ref[first:span, :] = jnp.dot(high, v, preferred_element_type=jnp.float32) + jnp.dot(
+            low_float.astype(jnp.bfloat16), v, preferred_element_type=jnp.float32
+        )
+        den = jnp.sum(high_float + low_float, axis=1, keepdims=True)
+        lane = lax.broadcasted_iota(jnp.int32, (tile, 128), 1)
+        aux_ref[first:span, :] = jnp.where(lane == 0, den, jnp.where(lane == 1, top, cum))
+
+    for copy in sends:
+        copy.wait()
+
+    pass_on(0, 2)
+    running = jnp.zeros((cut, width), jnp.float32)
+    vector = jnp.zeros((1, width), jnp.float32)
+    far_max = jnp.full((1, width), FLOOR_LOG, jnp.float32)
+    own_vector, own_max = vector, far_max
+    for step in range(count):
+        prefix_ref[step] = running
+        own_vector = jnp.where(place == step, vector, own_vector)
+        own_max = jnp.where(place == step, far_max, own_max)
+        if step < count - 1:
+            extra = extra_ref[step]
+            new_max, step_total = extra[2:3], extra[1:2]
+            joined = jnp.maximum(step_total + far_max, new_max)
+            keep_old = jnp.exp(step_total + far_max - joined)
+            keep_new = jnp.exp(new_max - joined)
+            running = keep_old * running + keep_new * piece_ref[step]
+            vector = keep_old * vector + keep_new * extra[0:1]
+            far_max = joined
+    backs = []
+    for step in range(1, count):
+        peer = lax.rem(place + step, count)
+        back = pltpu.make_async_remote_copy(
+            src_ref=prefix_ref.at[peer],
+            dst_ref=mat_ref.at[pl.ds(pl.multiple_of(place * cut, cut), cut)],
+            send_sem=back_send_sems.at[step - 1],
+            recv_sem=back_recv_sems.at[step - 1],
+            device_id={"sp": peer},
+            device_id_type=pl.DeviceIdType.MESH,
+        )
+        back.start()
+        backs.append(back)
+    mat_ref[pl.ds(pl.multiple_of(place * cut, cut), cut), :] = prefix_ref[place]
+
+    fetch(4, 8)
+    aux = aux_ref[...]
+    den, top, cum = aux[:, 0:1], aux[:, 1:2], aux[:, 2:3]
+    far = own_max[:, 0:1]
+    joined = jnp.maximum(top, far)
+    keep_own = jnp.exp(top - joined)
+    keep_far = jnp.exp(far - joined)
+    q_float = q_ref[...].astype(jnp.float32)
+    far_den = jnp.sum(q_float * own_vector, axis=1, keepdims=True)
+    denominator = keep_own * den + keep_far * far_den
+    divisor = jnp.maximum(jnp.abs(denominator), jnp.exp(-(cum + joined)))
+    pass_on(2, 4)
+    for copy in backs:
+        copy.wait()
+    one, rest = split_two(mat_ref[...])
+    two, three = split_two(mat_ref[...] - one.astype(jnp.float32))
+    q = q_ref[...]
+    far_num = (
+        jnp.dot(q, one, preferred_element_type=jnp.float32)
+        + jnp.dot(q, two, preferred_element_type=jnp.float32)
+        + jnp.dot(q, three, preferred_element_type=jnp.float32)
+    )
+    numerator = keep_own * num_ref[...] + keep_far * far_num
+    cell_ref[...] = (numerator / divisor).astype(cell_ref.dtype)
+
+    share = seq_len // heads
+    columns = pl.ds(pl.multiple_of(head * width, width), width)
+    turns = []
+    for step in range(1, heads):
+        peer = lax.rem(head + step, heads)
+        turn = pltpu.make_async_remote_copy(
+            src_ref=cell_ref.at[pl.ds(pl.multiple_of(peer * share, share), share)],
+            dst_ref=token_ref.at[:, columns],
+            send_sem=turn_send_sems.at[step - 1],
+            recv_sem=turn_recv_sems.at[step - 1],
+            device_id={"tp": peer},
+            device_id_type=pl.DeviceIdType.MESH,
+        )
+        turn.start()
+        turns.append(turn)
+    own_copy = pltpu.make_async_copy(
+        cell_ref.at[pl.ds(pl.multiple_of(head * share, share), share)],
+        token_ref.at[:, columns],
+        own_sem,
+    )
+    own_copy.start()
+    fetch(8, chunks)
+    for load in loads[:3]:
+        load.wait()
+    own_copy.wait()
+    for copy in turns:
+        copy.wait()
+
+    def row_copy(src, source, half, way):
+        unit = source * halves + half
+        return remote(
+            src,
+            held_ref.at[unit],
+            row_send.at[way, unit],
+            row_recv.at[unit],
+            place + (4 * way - 2),
+        )
+
+    def sum_copy(target, half, way, piece):
+        landing = ((target + way) * halves + half) * pieces + piece
+        leaving = (target * halves + half) * pieces + piece
+        return remote(
+            part_ref.at[leaving],
+            sum_ref.at[landing],
+            sum_send.at[leaving],
+            sum_recv.at[landing],
+            place + (4 * way - 2),
+        )
+
+    def sum_wait(landing):
+        remote(
+            part_ref.at[0], sum_ref.at[landing], sum_send.at[0], sum_recv.at[landing], twin
+        ).wait_recv()
+
+    for half in range(halves):
+        span = slice(half * tokens, (half + 1) * tokens)
+        cell_float = token_ref[span, :].astype(jnp.float32)
+        headed = (
+            cell_float
+            * lax.rsqrt(jnp.mean(cell_float * cell_float, axis=1, keepdims=True) + EPS)
+            * head_gain_ref[...]
+        )
+        gated = (headed * jax.nn.sigmoid(out_gate_ref[span, :].astype(jnp.float32))).astype(
+            jnp.bfloat16
+        )
+        mixed = resid_ref[span, :].astype(jnp.float32) + jnp.dot(
+            gated, out_proj_ref[...], preferred_element_type=jnp.float32
+        )
+        own_ref[half] = mixed
+        normed = (
+            mixed
+            * lax.rsqrt(jnp.mean(mixed * mixed, axis=1, keepdims=True) + EPS)
+            * ffn_gain_ref[...]
+        ).astype(jnp.bfloat16)
+        rows_ref[half] = normed
+        held_ref[here * halves + half] = normed
+        if half == 0:
+            for way in range(2):
+
+                @pl.when((here < last) if way else (here > 0))
+                def _():
+                    row_copy(rows_ref.at[0], here, 0, way).start()
+
+    def later_halves(way):
+        for half in range(1, halves):
+            row_copy(rows_ref.at[half], here, half, way).start()
+
+    @pl.when(here == 0)
+    def _():
+        later_halves(1)
+
+    @pl.when(here == last)
+    def _():
+        later_halves(0)
+
+    for step in range(1, line):
+        info_copy(step).wait()
+    for load in loads[3:]:
+        load.wait()
+
+    shorter = jnp.minimum(here, last - here)
+
+    def in_stream(p, reach):
+        first = p < reach
+        turn = p - reach
+        ahead = jnp.where(first, p + 1, reach - turn // (halves - 1))
+        return ahead, jnp.where(first, 0, 1 + lax.rem(turn, halves - 1))
+
+    def source_of(k):
+        p = k - halves
+        both = shorter * 2 * halves
+        paired = p < both
+        way = jnp.where(paired, lax.rem(p, 2), jnp.where(here < last - here, 1, 0))
+        spot = jnp.where(paired, p // 2, p - shorter * halves)
+        reach = jnp.where(way == 1, last - here, here)
+        ahead, half = in_stream(spot, reach)
+        is_own = k < halves
+        final = spot == reach * halves - 1
+        return (
+            jnp.where(is_own, here, here + ahead * (2 * way - 1)),
+            jnp.where(is_own, k, half),
+            final,
+        )
+
+    def matches(source, half, weighted):
+        info = infos_ref[source, half]
+        rank = lax.broadcasted_iota(jnp.int32, (slots, tokens), 0).astype(jnp.float32)
+        tables = []
+        for expert in (place, twin):
+            name = expert.astype(jnp.float32)
+            table = jnp.zeros((slots, tokens), jnp.float32)
+            for route in range(2):
+                hit = jnp.where(info[route : route + 1] == name, info[2 + route : 3 + route], -1.0)
+                value = info[4 + route : 5 + route] if weighted else 1.0
+                table += jnp.where(hit == rank, value, 0.0)
+            tables.append(table)
+        return jnp.concatenate(tables, axis=0)
+
+    first_way = jnp.where(last - here <= here, 0, 1)
+
+    def relay(way, spot):
+        reach = jnp.where(way == 1, last - here, here)
+
+        @pl.when((spot >= 0) & (spot < reach * halves) & (here > 0) & (here < last))
+        def _():
+            ahead, half = in_stream(spot, reach)
+            target = here + ahead * (2 * way - 1)
+            for piece in range(pieces):
+                unit = (target * halves + half) * pieces + piece
+                landing = ((target + way) * halves + half) * pieces + piece
+                sum_wait(landing)
+                part_ref[unit] = (
+                    part_ref[unit].astype(jnp.float32) + sum_ref[landing].astype(jnp.float32)
+                ).astype(jnp.bfloat16)
+                sum_copy(target, half, way, piece).start()
+
+    def expert(rows, gate_mat, up_mat, down_mat):
+        gate = jnp.dot(rows, gate_mat[...], preferred_element_type=jnp.float32)
+        up = jnp.dot(rows, up_mat[...], preferred_element_type=jnp.float32)
+        active = (jax.nn.silu(gate) * up).astype(jnp.bfloat16)
+        return jnp.dot(active, down_mat[...], preferred_element_type=jnp.float32).astype(
+            jnp.bfloat16
+        )
+
+    def combine(k, carry):
+        source, half, _ = source_of(jnp.where(k < units, k, k - units))
+        unit = source * halves + half
+        done_ref[unit, slots : 2 * slots, :] = expert(
+            cross_ref[unit], twin_gate_ref, twin_up_ref, twin_down_ref
+        )
+        high, low = split_two(matches(source, half, True))
+        answers = done_ref[unit]
+        turned = (((0,), (0,)), ((), ()))
+        part = lax.dot_general(
+            high, answers, turned, preferred_element_type=jnp.float32
+        ) + lax.dot_general(low, answers, turned, preferred_element_type=jnp.float32)
+
+        @pl.when(source == here)
+        def _():
+            own_ref[half] = own_ref[half] + part
+
+        @pl.when(source != here)
+        def _():
+            for piece in range(pieces):
+                part_ref[unit * pieces + piece] = part[
+                    piece * grain : (piece + 1) * grain
+                ].astype(jnp.bfloat16)
+
+        @pl.when((source < here) & (here == last))
+        def _():
+            for piece in range(pieces):
+                sum_copy(source, half, 0, piece).start()
+
+        @pl.when((source > here) & (here == 0))
+        def _():
+            for piece in range(pieces):
+                sum_copy(source, half, 1, piece).start()
+
+        return carry
+
+    ready = min(3, units - 1)
+
+    def step_body(k, carry):
+        @pl.when(k < units)
+        def _():
+            source, half, final = source_of(k)
+            unit = source * halves + half
+
+            @pl.when(source != here)
+            def _():
+                remote(
+                    held_ref.at[unit], held_ref.at[unit], row_send.at[0, unit], row_recv.at[unit], twin
+                ).wait_recv()
+
+            @pl.when((source < here) & (here < last))
+            def _():
+                row_copy(held_ref.at[unit], source, half, 1).start()
+
+                @pl.when(final)
+                def _():
+                    later_halves(1)
+
+            @pl.when((source > here) & (here > 0))
+            def _():
+                row_copy(held_ref.at[unit], source, half, 0).start()
+
+                @pl.when(final)
+                def _():
+                    later_halves(0)
+
+            packed = jnp.dot(
+                matches(source, half, False).astype(jnp.bfloat16),
+                held_ref[unit],
+                preferred_element_type=jnp.float32,
+            ).astype(jnp.bfloat16)
+            cross_ref[unit] = packed[slots:]
+            done_ref[unit, 0:slots, :] = expert(
+                packed[:slots], gate_ref.at[0], up_ref.at[0], down_ref.at[0]
+            )
+
+        @pl.when(k == 0)
+        def _():
+            pass_on(4, 8)
+            hand_over(0, 2)
+
+        @pl.when(k == 1)
+        def _():
+            pass_on(8, chunks)
+            hand_over(2, 6)
+
+        @pl.when(k == 2)
+        def _():
+            hand_over(6, 9)
+
+        @pl.when(k == ready)
+        def _():
+            hand_over(9, chunks)
+            for chunk in range(chunks):
+                weight_copy(2, chunk).wait_recv()
+                weight_copy(3, chunk).wait_recv()
+
+        relay(first_way, k - units)
+        relay(1 - first_way, k - units - 2)
+        low = jnp.where(k == ready, halves, k)
+        lax.fori_loop(low, jnp.where(k >= ready, k + 1, low), combine, 0)
+        return carry
+
+    lax.fori_loop(0, units + halves, step_body, 0)
+    for spot in range(halves, last * halves):
+        relay(first_way, spot)
+        relay(1 - first_way, spot - 2)
+
+    for half in range(halves):
+        for piece in range(pieces):
+            rows = pl.ds(piece * grain, grain)
+            for way in range(2):
+
+                @pl.when((here > 0) if way else (here < last))
+                def _():
+                    landing = ((here + way) * halves + half) * pieces + piece
+                    sum_wait(landing)
+                    own_ref[half, rows] = own_ref[half, rows] + sum_ref[landing].astype(jnp.float32)
+
+            out_ref[half, rows] = own_ref[half, rows].astype(out_ref.dtype)
+
+    def drain(unit, carry):
+        source = unit // halves
+        half = lax.rem(unit, halves)
+
+        @pl.when((source <= here) & (here < last))
+        def _():
+            row_copy(held_ref.at[unit], source, half, 1).wait_send()
+
+        @pl.when((source >= here) & (here > 0))
+        def _():
+            row_copy(held_ref.at[unit], source, half, 0).wait_send()
+
+        @pl.when(source != here)
+        def _():
+            for piece in range(pieces):
+                sum_copy(source, half, 0, piece).wait_send()
+
+        return carry
+
+    lax.fori_loop(0, units, drain, 0)
+    for chunk in range(chunks):
+        for stage in range(4):
+            weight_copy(stage, chunk).wait_send()
+
+
+def run_layer(
+    resid,
+    query,
+    keys,
+    values,
+    out_gate,
+    forget_pre,
+    input_pre,
+    head_gain,
+    out_proj,
+    ffn_gain,
+    routes,
+    route_scores,
+    w_gate,
+    w_up,
+    w_down,
+    halves,
+    slots,
+):
+    count, heads = lax.axis_size("sp"), lax.axis_size("tp")
+    line = count // 2
+    units = line * halves
+    seq_len, width = query.shape
+    cut = width // count
+    share = seq_len // heads
+    wide = resid.shape[1]
+    tokens = share // halves
+    pieces = 2
+    grain = tokens // pieces
+    tile = 4 * BLOCK if seq_len % (4 * BLOCK) == 0 else BLOCK
+    vmem = pl.BlockSpec(memory_space=pltpu.VMEM)
+    whole = pl.BlockSpec(memory_space=pl.ANY)
+    dma = pltpu.SemaphoreType.DMA
+    f32, bf16 = jnp.float32, jnp.bfloat16
+    chunks = 3 * WEIGHT_PIECES
+    out = pl.pallas_call(
+        functools.partial(
+            layer_kernel,
+            count=count,
+            heads=heads,
+            line=line,
+            halves=halves,
+            slots=slots,
+            pieces=pieces,
+            tile=tile,
+        ),
+        out_shape=jax.ShapeDtypeStruct((halves, tokens, wide), bf16),
+        in_specs=[vmem] * 9 + [whole] * 6,
+        out_specs=vmem,
+        scratch_shapes=[
+            pltpu.VMEM((width + EXTRA, width), f32),
+            pltpu.VMEM((count, cut, width), f32),
+            pltpu.VMEM((count, EXTRA, width), f32),
+            pltpu.VMEM((count, cut, width), f32),
+            pltpu.VMEM((width, width), f32),
+            pltpu.VMEM((seq_len, width), f32),
+            pltpu.VMEM((seq_len, 128), f32),
+            pltpu.VMEM((seq_len, width), bf16),
+            pltpu.VMEM((share, heads * width), bf16),
+            pltpu.VMEM(resid.shape, bf16),
+            pltpu.VMEM(out_gate.shape, bf16),
+            pltpu.VMEM(out_proj.shape, bf16),
+            pltpu.VMEM(w_gate.shape, bf16),
+            pltpu.VMEM(w_up.shape, bf16),
+            pltpu.VMEM(w_down.shape, bf16),
+            pltpu.VMEM(w_gate.shape[1:], bf16),
+            pltpu.VMEM(w_up.shape[1:], bf16),
+            pltpu.VMEM(w_down.shape[1:], bf16),
+            pltpu.VMEM((line, halves, 8, tokens), f32),
+            pltpu.VMEM((halves, tokens, wide), bf16),
+            pltpu.VMEM((units, tokens, wide), bf16),
+            pltpu.VMEM((units, slots, wide), bf16),
+            pltpu.VMEM((units, 2 * slots, wide), bf16),
+            pltpu.VMEM((units * pieces, grain, wide), bf16),
+            pltpu.VMEM((halves, tokens, wide), f32),
+            pltpu.VMEM(((units + halves) * pieces, grain, wide), bf16),
+            dma((6,)),
+            dma(()),
+            dma((count - 1,)),
+            dma((count - 1,)),
+            dma((count - 1,)),
+            dma((count - 1,)),
+            dma((count - 1,)),
+            dma((count - 1,)),
+            dma((heads - 1,)),
+            dma((heads - 1,)),
+            dma((line - 1,)),
+            dma((line - 1,)),
+            dma((2, units)),
+            dma((units,)),
+            dma((units * pieces,)),
+            dma(((units + halves) * pieces,)),
+            dma((4, chunks)),
+            dma((4, chunks)),
+        ],
+        compiler_params=pltpu.CompilerParams(
+            vmem_limit_bytes=LAYER_VMEM, collective_id=5, has_side_effects=True
+        ),
+        cost_estimate=pl.CostEstimate(flops=10**10, bytes_accessed=2**24, transcendentals=0),
+        name="layer",
+    )(
+        query,
+        keys,
+        values,
+        forget_pre,
+        input_pre,
+        head_gain[None, :],
+        ffn_gain[None, :],
+        routes.T,
+        route_scores.T,
+        resid,
+        out_gate,
+        out_proj,
+        w_gate,
+        w_up,
+        w_down,
+    )
+    return out.reshape(share, wide)
 
 
 def slot_select(expert_ids, expert_count, capacity):
@@ -975,6 +1737,28 @@
     expert_count = local_experts * sources
     half_rows = row_count // 2
     capacity = max(2, 2 * half_rows * route_count // expert_count)
+    dense = local_experts == 1 and sources % 2 == 0 and sources <= 8 and route_count == 2
+    dense = dense and 2 * capacity >= half_rows and capacity % 16 == 0 and half_rows % 32 == 0
+    if dense and lax.axis_size("tp") == 4 and head_width % (8 * sources) == 0:
+        return run_layer(
+            resid,
+            query,
+            keys,
+            values,
+            out_gate,
+            forget_pre,
+            input_pre,
+            head_gain,
+            out_proj,
+            ffn_gain,
+            routes,
+            route_scores,
+            w_gate,
+            w_up,
+            w_down,
+            2,
+            capacity,
+        )
     route_weight = route_scores / jnp.sum(route_scores, axis=1, keepdims=True)
     token_rows = token_cell(query, keys, values, forget_pre, input_pre)
     cell_float = token_rows.astype(jnp.float32)
@@ -992,8 +1776,7 @@
         * lax.rsqrt(jnp.mean(after_mix * after_mix, axis=1, keepdims=True) + EPS)
         * ffn_gain[None, :]
     ).astype(jnp.bfloat16)
-    dense = local_experts == 1 and sources % 2 == 0 and sources <= 8 and route_count == 2
-    if dense and 2 * capacity >= half_rows and capacity % 16 == 0 and half_rows % 32 == 0:
+    if dense:
         info = route_info(routes, route_weight, 2)
         return run_line(normed_rows, after_mix, info, w_gate, w_up, w_down, capacity)
     selects = [

time: 139 us -> 129 us (0.928)
  other arithmetic: 5.46 us -> 0 us
  matrix products: 2.29 us -> 0 us
  local copies, waits for them, and re-layouts: 3.64 us -> 2.09 us
    dot_general x1 -> x0, matrix products: 2.29 us -> none  [shards(): jnp.dot(gated_out, out_proj, preferred_element_type=jnp.float32)]
    reduce_sum x3 -> x0, other arithmetic: 2.12 us -> none  [the longest x1 1.15 us: shards(): jnp.mean(cell_float * cell_float, axis=1, keepdims=True) + EPS]
    convert_element_type x2 -> x0, other arithmetic: 1.95 us -> none  [the longest x1 1.26 us: shards(): normed_rows = (after_mix * lax.rsqrt(jnp.mean(after_mix * after_mix, axis...]
    pallas_call x2 -> x1, Pallas kernels: 127 us -> 126 us  [run_layer(): pl.pallas_call(functools.partial(layer_kernel, count=count, heads=heads,...]
    unnamed x14 -> x1, local copies, waits for them, and re-layouts: 3.03 us -> 2.09 us
where the time goes in v4:
time: 129 us; the launch traced here: 128 us
  Pallas kernels  126 us (98%)
  local copies, waits for them, and re-layouts  2.09 us (2%)
    pallas_call x1, Pallas kernels, run_layer(): pl.pallas_call(functools.partial(layer_kernel, count=count, heads=heads,...  126 us

profile of v4, /device:TPU:0, one launch (start us, length us, event | category | flops | bytes accessed | tf_op | source)
XLA Modules:
  0.0 127.9 jit_solution(2850165647738677187)
XLA Ops:
  0.0 125.8 %layer.1 = bf16[2,96,2048]{2,1,0:T(8,128)(2,1)} custom-call(bf16[768,256]{1,0:T(8,128)(2,1)} %q_ref.1, bf16[768,256]{1,0:T(8,128)(2,1)} %k_ref.1, bf16[768,256]{1,0:T(8,128)(2,1)} %v_ref.1, f32[1,768]{1,0:T(1,128)} %forget_ref.1, f32[1,768]{1,0:T(1,128)} %input_ref.1, f32[1,1024]{1,0:T(1,128)} %bitcast.7, f32[1,2048]{1,0:T(1,128)} %bitcast.6, ...), custom_call_target="tpu_custom_call" | custom-call | flops 10000000000 | bytes 16777216 | tf_op jit(solution)/shard_map/layer/pallas_call | solution.py:1111
  125.8 2.1 %copy.17 = bf16[192,2048]{1,0:T(8,128)(2,1)} copy(bf16[192,2048]{1,0:T(8,128)(2,1)} %bitcast.5) | data formatting | bytes 1572864

commit v5 on v4

--- a/solution.py
+++ b/solution.py
@@ -465,13 +465,15 @@
     gate_ref,
     up_ref,
     down_ref,
-    twin_gate_ref,
-    twin_up_ref,
     twin_down_ref,
     infos_ref,
     rows_ref,
     held_ref,
     cross_ref,
+    crossed_ref,
+    answer_ref,
+    back_ref,
+    batch_ref,
     done_ref,
     part_ref,
     own_ref,
@@ -490,6 +492,10 @@
     info_recv,
     row_send,
     row_recv,
+    cross_send,
+    cross_recv,
+    answer_send,
+    answer_recv,
     sum_send,
     sum_recv,
     weight_send,
@@ -517,7 +523,7 @@
     grain = tokens // pieces
     last = line - 1
     shares = WEIGHT_PIECES
-    chunks = 3 * shares
+    chunks = shares
 
     def remote(src, dst, send, recv, peer, axis="sp"):
         return pltpu.make_async_remote_copy(
@@ -549,13 +555,10 @@
     greeted = sp_tp_barrier(barrier, {"sp": count, "tp": heads})
 
     def weight_rows(chunk, owner):
-        source = (gate_hbm, up_hbm, down_hbm)[chunk // shares]
-        target = (twin_gate_ref, twin_up_ref, twin_down_ref)[chunk // shares]
-        quarter = target.shape[0] // heads
+        quarter = twin_down_ref.shape[0] // heads
         size = quarter // shares
-        start = owner * quarter + (chunk % shares) * size
-        rows = pl.ds(pl.multiple_of(start, size), size)
-        return source.at[0, rows], target.at[rows]
+        rows = pl.ds(pl.multiple_of(owner * quarter + chunk * size, size), size)
+        return down_hbm.at[0, rows], twin_down_ref.at[rows]
 
     def weight_copy(stage, chunk):
         owner, peer, axis = (
@@ -626,7 +629,6 @@
 
     log_forget, cum_row, gap_row = log_rows(forget_ref, input_ref)
     pl.semaphore_wait(barrier, greeted)
-    fetch(0, 2)
     total = jnp.sum(log_forget, axis=1, keepdims=True)
     best = jnp.max(gap_row, axis=1, keepdims=True)
     keep_row = jnp.exp(gap_row - best) * width ** (-0.5)
@@ -674,8 +676,8 @@
     extra_ref[place] = state_ref[width : width + EXTRA, :]
     piece_ref[place] = state_ref[pl.ds(pl.multiple_of(place * cut, cut), cut), :]
 
-    fetch(2, 4)
-
+
+    fetch(0, 2)
     for first in range(0, seq_len, tile):
         span = first + tile
         row, col = col_mask(first, tile, span)
@@ -705,7 +707,6 @@
     for copy in sends:
         copy.wait()
 
-    pass_on(0, 2)
     running = jnp.zeros((cut, width), jnp.float32)
     vector = jnp.zeros((1, width), jnp.float32)
     far_max = jnp.full((1, width), FLOOR_LOG, jnp.float32)
@@ -738,7 +739,7 @@
         backs.append(back)
     mat_ref[pl.ds(pl.multiple_of(place * cut, cut), cut), :] = prefix_ref[place]
 
-    fetch(4, 8)
+    fetch(2, chunks)
     aux = aux_ref[...]
     den, top, cum = aux[:, 0:1], aux[:, 1:2], aux[:, 2:3]
     far = own_max[:, 0:1]
@@ -749,7 +750,6 @@
     far_den = jnp.sum(q_float * own_vector, axis=1, keepdims=True)
     denominator = keep_own * den + keep_far * far_den
     divisor = jnp.maximum(jnp.abs(denominator), jnp.exp(-(cum + joined)))
-    pass_on(2, 4)
     for copy in backs:
         copy.wait()
     one, rest = split_two(mat_ref[...])
@@ -784,12 +784,12 @@
         own_sem,
     )
     own_copy.start()
-    fetch(8, chunks)
     for load in loads[:3]:
         load.wait()
     own_copy.wait()
     for copy in turns:
         copy.wait()
+    pass_on(0, chunks)
 
     def row_copy(src, source, half, way):
         unit = source * halves + half
@@ -799,6 +799,24 @@
             row_send.at[way, unit],
             row_recv.at[unit],
             place + (4 * way - 2),
+        )
+
+    def cross_copy(unit):
+        return remote(
+            cross_ref.at[unit],
+            crossed_ref.at[unit],
+            cross_send.at[unit],
+            cross_recv.at[unit],
+            twin,
+        )
+
+    def answer_copy(unit):
+        return remote(
+            answer_ref.at[unit],
+            back_ref.at[unit],
+            answer_send.at[unit],
+            answer_recv.at[unit],
+            twin,
         )
 
     def sum_copy(target, half, way, piece):
@@ -860,9 +878,6 @@
 
     for step in range(1, line):
         info_copy(step).wait()
-    for load in loads[3:]:
-        load.wait()
-
     shorter = jnp.minimum(here, last - here)
 
     def in_stream(p, reach):
@@ -919,51 +934,16 @@
                 ).astype(jnp.bfloat16)
                 sum_copy(target, half, way, piece).start()
 
-    def expert(rows, gate_mat, up_mat, down_mat):
-        gate = jnp.dot(rows, gate_mat[...], preferred_element_type=jnp.float32)
-        up = jnp.dot(rows, up_mat[...], preferred_element_type=jnp.float32)
-        active = (jax.nn.silu(gate) * up).astype(jnp.bfloat16)
-        return jnp.dot(active, down_mat[...], preferred_element_type=jnp.float32).astype(
-            jnp.bfloat16
-        )
-
-    def combine(k, carry):
-        source, half, _ = source_of(jnp.where(k < units, k, k - units))
-        unit = source * halves + half
-        done_ref[unit, slots : 2 * slots, :] = expert(
-            cross_ref[unit], twin_gate_ref, twin_up_ref, twin_down_ref
-        )
-        high, low = split_two(matches(source, half, True))
-        answers = done_ref[unit]
-        turned = (((0,), (0,)), ((), ()))
-        part = lax.dot_general(
-            high, answers, turned, preferred_element_type=jnp.float32
-        ) + lax.dot_general(low, answers, turned, preferred_element_type=jnp.float32)
-
-        @pl.when(source == here)
-        def _():
-            own_ref[half] = own_ref[half] + part
-
-        @pl.when(source != here)
-        def _():
-            for piece in range(pieces):
-                part_ref[unit * pieces + piece] = part[
-                    piece * grain : (piece + 1) * grain
-                ].astype(jnp.bfloat16)
-
-        @pl.when((source < here) & (here == last))
-        def _():
-            for piece in range(pieces):
-                sum_copy(source, half, 0, piece).start()
-
-        @pl.when((source > here) & (here == 0))
-        def _():
-            for piece in range(pieces):
-                sum_copy(source, half, 1, piece).start()
-
-        return carry
-
-    ready = min(3, units - 1)
+    def down(active, mat):
+        return jnp.dot(active, mat, preferred_element_type=jnp.float32).astype(jnp.bfloat16)
+
+    def activate(rows):
+        gate = jnp.dot(rows, gate_ref[0], preferred_element_type=jnp.float32)
+        up = jnp.dot(rows, up_ref[0], preferred_element_type=jnp.float32)
+        return (jax.nn.silu(gate) * up).astype(jnp.bfloat16)
+
+    inner_stop = (here > 0) & (here < last)
+    lag = jnp.where(inner_stop, 1, 0)
 
     def step_body(k, carry):
         @pl.when(k < units)
@@ -999,41 +979,83 @@
                 preferred_element_type=jnp.float32,
             ).astype(jnp.bfloat16)
             cross_ref[unit] = packed[slots:]
-            done_ref[unit, 0:slots, :] = expert(
-                packed[:slots], gate_ref.at[0], up_ref.at[0], down_ref.at[0]
+            cross_copy(unit).start()
+            batch_ref[...] = packed[:slots]
+
+        @pl.when(k == 0)
+        def _():
+            for load in loads[3:]:
+                load.wait()
+
+        @pl.when(k == 1)
+        def _():
+            hand_over(0, chunks)
+
+        @pl.when(k < units)
+        def _():
+            source, half, _ = source_of(k)
+            done_ref[source * halves + half, 0:slots, :] = down(
+                activate(batch_ref[...]), down_ref[0]
             )
 
-        @pl.when(k == 0)
-        def _():
-            pass_on(4, 8)
-            hand_over(0, 2)
-
-        @pl.when(k == 1)
-        def _():
-            pass_on(8, chunks)
-            hand_over(2, 6)
-
-        @pl.when(k == 2)
-        def _():
-            hand_over(6, 9)
-
-        @pl.when(k == ready)
-        def _():
-            hand_over(9, chunks)
+        @pl.when(k == 1 + halves)
+        def _():
             for chunk in range(chunks):
                 weight_copy(2, chunk).wait_recv()
                 weight_copy(3, chunk).wait_recv()
 
+        def answer_twin():
+            source, half, _ = source_of(k - lag)
+            unit = source * halves + half
+            cross_copy(unit).wait_recv()
+            answer_ref[unit] = activate(crossed_ref[unit])
+            answer_copy(unit).start()
+
+        pl.when(inner_stop & (k >= lag) & (k < units + lag))(answer_twin)
+
         relay(first_way, k - units)
         relay(1 - first_way, k - units - 2)
-        low = jnp.where(k == ready, halves, k)
-        lax.fori_loop(low, jnp.where(k >= ready, k + 1, low), combine, 0)
+        turn_now = k - 1 - lag
+
+        @pl.when((turn_now >= halves) & (turn_now < units + halves))
+        def _():
+            source, half, _ = source_of(jnp.where(turn_now < units, turn_now, turn_now - units))
+            unit = source * halves + half
+            answer_copy(unit).wait_recv()
+            done_ref[unit, slots : 2 * slots, :] = down(back_ref[unit], twin_down_ref[...])
+            high, low = split_two(matches(source, half, True))
+            answers = done_ref[unit]
+            turned = (((0,), (0,)), ((), ()))
+            part = lax.dot_general(
+                high, answers, turned, preferred_element_type=jnp.float32
+            ) + lax.dot_general(low, answers, turned, preferred_element_type=jnp.float32)
+
+            @pl.when(source == here)
+            def _():
+                own_ref[half] = own_ref[half] + part
+
+            @pl.when(source != here)
+            def _():
+                for piece in range(pieces):
+                    part_ref[unit * pieces + piece] = part[
+                        piece * grain : (piece + 1) * grain
+                    ].astype(jnp.bfloat16)
+
+            @pl.when((source < here) & (here == last))
+            def _():
+                for piece in range(pieces):
+                    sum_copy(source, half, 0, piece).start()
+
+            @pl.when((source > here) & (here == 0))
+            def _():
+                for piece in range(pieces):
+                    sum_copy(source, half, 1, piece).start()
+
+        pl.when(~inner_stop & (k < units))(answer_twin)
+
         return carry
 
-    lax.fori_loop(0, units + halves, step_body, 0)
-    for spot in range(halves, last * halves):
-        relay(first_way, spot)
-        relay(1 - first_way, spot - 2)
+    lax.fori_loop(0, units + 2 + halves, step_body, 0)
 
     for half in range(halves):
         for piece in range(pieces):
@@ -1051,6 +1073,8 @@
     def drain(unit, carry):
         source = unit // halves
         half = lax.rem(unit, halves)
+        cross_copy(unit).wait_send()
+        answer_copy(unit).wait_send()
 
         @pl.when((source <= here) & (here < last))
         def _():
@@ -1098,7 +1122,7 @@
     seq_len, width = query.shape
     cut = width // count
     share = seq_len // heads
-    wide = resid.shape[1]
+    wide, inner = resid.shape[1], w_down.shape[1]
     tokens = share // halves
     pieces = 2
     grain = tokens // pieces
@@ -1107,7 +1131,7 @@
     whole = pl.BlockSpec(memory_space=pl.ANY)
     dma = pltpu.SemaphoreType.DMA
     f32, bf16 = jnp.float32, jnp.bfloat16
-    chunks = 3 * WEIGHT_PIECES
+    chunks = WEIGHT_PIECES
     out = pl.pallas_call(
         functools.partial(
             layer_kernel,
@@ -1138,13 +1162,15 @@
             pltpu.VMEM(w_gate.shape, bf16),
             pltpu.VMEM(w_up.shape, bf16),
             pltpu.VMEM(w_down.shape, bf16),
-            pltpu.VMEM(w_gate.shape[1:], bf16),
-            pltpu.VMEM(w_up.shape[1:], bf16),
             pltpu.VMEM(w_down.shape[1:], bf16),
             pltpu.VMEM((line, halves, 8, tokens), f32),
             pltpu.VMEM((halves, tokens, wide), bf16),
             pltpu.VMEM((units, tokens, wide), bf16),
             pltpu.VMEM((units, slots, wide), bf16),
+            pltpu.VMEM((units, slots, wide), bf16),
+            pltpu.VMEM((units, slots, inner), bf16),
+            pltpu.VMEM((units, slots, inner), bf16),
+            pltpu.VMEM((slots, wide), bf16),
             pltpu.VMEM((units, 2 * slots, wide), bf16),
             pltpu.VMEM((units * pieces, grain, wide), bf16),
             pltpu.VMEM((halves, tokens, wide), f32),
@@ -1162,6 +1188,10 @@
             dma((line - 1,)),
             dma((line - 1,)),
             dma((2, units)),
+            dma((units,)),
+            dma((units,)),
+            dma((units,)),
+            dma((units,)),
             dma((units,)),
             dma((units * pieces,)),
             dma(((units + halves) * pieces,)),

time: 129 us -> 120 us (0.930); the launches traced: 128 us -> 120 us
  Pallas kernels: 126 us -> 118 us
    pallas_call x1, Pallas kernels: 126 us -> 118 us  [run_layer(): pl.pallas_call(functools.partial(layer_kernel, count=count, heads=heads,...]
where the time goes in v5:
time: 120 us
  Pallas kernels  118 us (98%)
  local copies, waits for them, and re-layouts  2.09 us (2%)
    pallas_call x1, Pallas kernels, run_layer(): pl.pallas_call(functools.partial(layer_kernel, count=count, heads=heads,...  118 us

profile of v5, /device:TPU:0, one launch (start us, length us, event | category | flops | bytes accessed | tf_op | source)
XLA Modules:
  0.0 120.2 jit_solution(6432845896439460961)
XLA Ops:
  0.0 118.1 %layer.1 = bf16[2,96,2048]{2,1,0:T(8,128)(2,1)} custom-call(bf16[768,256]{1,0:T(8,128)(2,1)} %q_ref.1, bf16[768,256]{1,0:T(8,128)(2,1)} %k_ref.1, bf16[768,256]{1,0:T(8,128)(2,1)} %v_ref.1, f32[1,768]{1,0:T(1,128)} %forget_ref.1, f32[1,768]{1,0:T(1,128)} %input_ref.1, f32[1,1024]{1,0:T(1,128)} %bitcast.7, f32[1,2048]{1,0:T(1,128)} %bitcast.6, ...), custom_call_target="tpu_custom_call" | custom-call | flops 10000000000 | bytes 16777216 | tf_op jit(solution)/shard_map/layer/pallas_call | solution.py:1135
  118.2 2.1 %copy.17 = bf16[192,2048]{1,0:T(8,128)(2,1)} copy(bf16[192,2048]{1,0:T(8,128)(2,1)} %bitcast.5) | data formatting | bytes 1572864

commit v6 on v5

--- a/solution.py
+++ b/solution.py
@@ -602,6 +602,54 @@
             peer * 2 + side,
         )
 
+    log_forget, cum_row, gap_row = log_rows(forget_ref, input_ref)
+    pl.semaphore_wait(barrier, greeted)
+    total = jnp.sum(log_forget, axis=1, keepdims=True)
+    best = jnp.max(gap_row, axis=1, keepdims=True)
+    keep_row = jnp.exp(gap_row - best) * width ** (-0.5)
+    weighted = k_ref[...].astype(jnp.float32).T * keep_row
+    high, low = split_two(weighted)
+    v_all = v_ref[...]
+    state_ref[0:width, :] = jnp.dot(high, v_all, preferred_element_type=jnp.float32) + jnp.dot(
+        low, v_all, preferred_element_type=jnp.float32
+    )
+    vector = jnp.dot(
+        jnp.broadcast_to(keep_row, (8, seq_len)),
+        k_ref[...].astype(jnp.float32),
+        precision=HIGHEST,
+        preferred_element_type=jnp.float32,
+    )[0:1]
+    lanes = jnp.zeros((1, width), jnp.float32)
+    state_ref[width : width + EXTRA, :] = jnp.concatenate(
+        [vector, lanes + total, lanes + total + best, jnp.zeros((EXTRA - 3, width), jnp.float32)],
+        axis=0,
+    )
+    sends = []
+    for step in range(1, count):
+        peer = lax.rem(place + step, count)
+        extra_copy = pltpu.make_async_remote_copy(
+            src_ref=state_ref.at[pl.ds(width, EXTRA)],
+            dst_ref=extra_ref.at[place],
+            send_sem=extra_send_sems.at[step - 1],
+            recv_sem=extra_recv_sems.at[step - 1],
+            device_id={"sp": peer},
+            device_id_type=pl.DeviceIdType.MESH,
+        )
+        piece_copy = pltpu.make_async_remote_copy(
+            src_ref=state_ref.at[pl.ds(pl.multiple_of(peer * cut, cut), cut)],
+            dst_ref=piece_ref.at[place],
+            send_sem=send_sems.at[step - 1],
+            recv_sem=recv_sems.at[step - 1],
+            device_id={"sp": peer},
+            device_id_type=pl.DeviceIdType.MESH,
+        )
+        extra_copy.start()
+        piece_copy.start()
+        sends += [extra_copy, piece_copy]
+    extra_ref[place] = state_ref[width : width + EXTRA, :]
+    piece_ref[place] = state_ref[pl.ds(pl.multiple_of(place * cut, cut), cut), :]
+
+
     eye_row, eye_col = col_mask(0, tokens, tokens)
     eye = jnp.where(eye_row == eye_col, 1.0, 0.0)
     for half in range(halves):
@@ -627,57 +675,9 @@
             [ids] + ranks + [scores / jnp.sum(scores, axis=0, keepdims=True), zeros[0:2]], axis=0
         )
 
-    log_forget, cum_row, gap_row = log_rows(forget_ref, input_ref)
-    pl.semaphore_wait(barrier, greeted)
-    total = jnp.sum(log_forget, axis=1, keepdims=True)
-    best = jnp.max(gap_row, axis=1, keepdims=True)
-    keep_row = jnp.exp(gap_row - best) * width ** (-0.5)
-    weighted = k_ref[...].astype(jnp.float32).T * keep_row
-    high, low = split_two(weighted)
-    v_all = v_ref[...]
-    state_ref[0:width, :] = jnp.dot(high, v_all, preferred_element_type=jnp.float32) + jnp.dot(
-        low, v_all, preferred_element_type=jnp.float32
-    )
-    vector = jnp.dot(
-        jnp.broadcast_to(keep_row, (8, seq_len)),
-        k_ref[...].astype(jnp.float32),
-        precision=HIGHEST,
-        preferred_element_type=jnp.float32,
-    )[0:1]
-    lanes = jnp.zeros((1, width), jnp.float32)
-    state_ref[width : width + EXTRA, :] = jnp.concatenate(
-        [vector, lanes + total, lanes + total + best, jnp.zeros((EXTRA - 3, width), jnp.float32)],
-        axis=0,
-    )
     for step in range(1, line):
         info_copy(step).start()
-    sends = []
-    for step in range(1, count):
-        peer = lax.rem(place + step, count)
-        extra_copy = pltpu.make_async_remote_copy(
-            src_ref=state_ref.at[pl.ds(width, EXTRA)],
-            dst_ref=extra_ref.at[place],
-            send_sem=extra_send_sems.at[step - 1],
-            recv_sem=extra_recv_sems.at[step - 1],
-            device_id={"sp": peer},
-            device_id_type=pl.DeviceIdType.MESH,
-        )
-        piece_copy = pltpu.make_async_remote_copy(
-            src_ref=state_ref.at[pl.ds(pl.multiple_of(peer * cut, cut), cut)],
-            dst_ref=piece_ref.at[place],
-            send_sem=send_sems.at[step - 1],
-            recv_sem=recv_sems.at[step - 1],
-            device_id={"sp": peer},
-            device_id_type=pl.DeviceIdType.MESH,
-        )
-        extra_copy.start()
-        piece_copy.start()
-        sends += [extra_copy, piece_copy]
-    extra_ref[place] = state_ref[width : width + EXTRA, :]
-    piece_ref[place] = state_ref[pl.ds(pl.multiple_of(place * cut, cut), cut), :]
-
-
-    fetch(0, 2)
+
     for first in range(0, seq_len, tile):
         span = first + tile
         row, col = col_mask(first, tile, span)
@@ -739,7 +739,6 @@
         backs.append(back)
     mat_ref[pl.ds(pl.multiple_of(place * cut, cut), cut), :] = prefix_ref[place]
 
-    fetch(2, chunks)
     aux = aux_ref[...]
     den, top, cum = aux[:, 0:1], aux[:, 1:2], aux[:, 2:3]
     far = own_max[:, 0:1]
@@ -784,12 +783,12 @@
         own_sem,
     )
     own_copy.start()
+    fetch(0, chunks)
     for load in loads[:3]:
         load.wait()
     own_copy.wait()
     for copy in turns:
         copy.wait()
-    pass_on(0, chunks)
 
     def row_copy(src, source, half, way):
         unit = source * halves + half
@@ -945,33 +944,43 @@
     inner_stop = (here > 0) & (here < last)
     lag = jnp.where(inner_stop, 1, 0)
 
-    def step_body(k, carry):
-        @pl.when(k < units)
-        def _():
-            source, half, final = source_of(k)
-            unit = source * halves + half
-
-            @pl.when(source != here)
+    def row_wait(unit):
+        remote(
+            held_ref.at[unit], held_ref.at[unit], row_send.at[0, unit], row_recv.at[unit], twin
+        ).wait_recv()
+
+    def forward(k):
+        source, half, final = source_of(k)
+        unit = source * halves + half
+        row_wait(unit)
+        for way in range(2):
+
+            @pl.when((source < here) if way else (source > here))
             def _():
-                remote(
-                    held_ref.at[unit], held_ref.at[unit], row_send.at[0, unit], row_recv.at[unit], twin
-                ).wait_recv()
-
-            @pl.when((source < here) & (here < last))
-            def _():
-                row_copy(held_ref.at[unit], source, half, 1).start()
+                row_copy(held_ref.at[unit], source, half, way).start()
 
                 @pl.when(final)
                 def _():
-                    later_halves(1)
-
-            @pl.when((source > here) & (here > 0))
+                    later_halves(way)
+
+    def forward_now(k):
+        spot = k - halves
+        paired = spot < shorter * 2 * halves
+        leads = (spot >= 0) & (jnp.where(paired, lax.rem(spot, 2), 0) == 0)
+        pl.when(inner_stop & leads)(lambda: forward(k))
+        pl.when(inner_stop & leads & paired)(lambda: forward(k + 1))
+
+    def step_body(k, carry):
+        pl.when(k < units)(lambda: forward_now(k))
+
+        @pl.when(k < units)
+        def _():
+            source, half, _ = source_of(k)
+            unit = source * halves + half
+
+            @pl.when((source != here) & ~inner_stop)
             def _():
-                row_copy(held_ref.at[unit], source, half, 0).start()
-
-                @pl.when(final)
-                def _():
-                    later_halves(0)
+                row_wait(unit)
 
             packed = jnp.dot(
                 matches(source, half, False).astype(jnp.bfloat16),
@@ -989,7 +998,7 @@
 
         @pl.when(k == 1)
         def _():
-            hand_over(0, chunks)
+            pass_on(0, chunks)
 
         @pl.when(k < units)
         def _():
@@ -997,6 +1006,10 @@
             done_ref[source * halves + half, 0:slots, :] = down(
                 activate(batch_ref[...]), down_ref[0]
             )
+
+        @pl.when(k == 2)
+        def _():
+            hand_over(0, chunks)
 
         @pl.when(k == 1 + halves)
         def _():

time: 120 us -> 116 us (0.967)
  Pallas kernels: 118 us -> 114 us
    pallas_call x1, Pallas kernels: 118 us -> 114 us  [run_layer(): pl.pallas_call(functools.partial(layer_kernel, count=count, heads=heads,...]
where the time goes in v6:
time: 116 us
  Pallas kernels  114 us (98%)
  local copies, waits for them, and re-layouts  2.09 us (2%)
    pallas_call x1, Pallas kernels, run_layer(): pl.pallas_call(functools.partial(layer_kernel, count=count, heads=heads,...  114 us

profile of v6, /device:TPU:0, one launch (start us, length us, event | category | flops | bytes accessed | tf_op | source)
XLA Modules:
  0.0 115.7 jit_solution(12624155670297096400)
XLA Ops:
  0.0 113.6 %layer.1 = bf16[2,96,2048]{2,1,0:T(8,128)(2,1)} custom-call(bf16[768,256]{1,0:T(8,128)(2,1)} %q_ref.1, bf16[768,256]{1,0:T(8,128)(2,1)} %k_ref.1, bf16[768,256]{1,0:T(8,128)(2,1)} %v_ref.1, f32[1,768]{1,0:T(1,128)} %forget_ref.1, f32[1,768]{1,0:T(1,128)} %input_ref.1, f32[1,1024]{1,0:T(1,128)} %bitcast.7, f32[1,2048]{1,0:T(1,128)} %bitcast.6, ...), custom_call_target="tpu_custom_call" | custom-call | flops 10000000000 | bytes 16777216 | tf_op jit(solution)/shard_map/layer/pallas_call | solution.py:1148
  113.7 2.1 %copy.17 = bf16[192,2048]{1,0:T(8,128)(2,1)} copy(bf16[192,2048]{1,0:T(8,128)(2,1)} %bitcast.5) | data formatting | bytes 1572864
